TPU v7x, 256 devices: a whole 4x4x8 slice. The times are simulated.
256 devices in a mesh: ep: 128 (over z, y, x), tp: 2 (over core).
Axes of the slice: x: 4, y: 4, z: 8, core: 2. Of those that a mesh axis runs over, the one named last changes fastest.
Arguments:
- tokens: bfloat16 [256, 2048], P('ep'), may hold values from -6 to 6
- head_state: float32 [256, 32, 64, 128], P('ep', 'tp'), may hold values from -4 to 4
- conv_state: bfloat16 [256, 3, 2048], P('ep', None, 'tp'), may hold values from -6 to 6
- conv_proj_state: bfloat16 [256, 3, 2, 512], P('ep', None, None, 'tp'), may hold values from -6 to 6
- first_gain: float32 [2048], replicated, may hold values from 0.1 to 1.9
- gate_weight: bfloat16 [2048, 2048], P('ep', 'tp'), may hold values from -0.125 to 0.125
- inner_weight: bfloat16 [2048, 2048], P('ep', 'tp'), may hold values from -0.125 to 0.125
- write_weight: bfloat16 [2048, 512], P(None, 'tp'), may hold values from -0.125 to 0.125
- read_weight: bfloat16 [2048, 512], P(None, 'tp'), may hold values from -0.125 to 0.125
- step_weight: bfloat16 [2048, 32], P(None, 'tp'), may hold values from -0.125 to 0.125
- conv_kernel: float32 [4, 2048], P(None, 'tp'), may hold values from -3 to 3
- conv_proj_kernel: float32 [4, 2, 512], P(None, None, 'tp'), may hold values from -3 to 3
- step_bias: float32 [32], P('tp'), may hold values from -2 to 1
- log_rate: float32 [32], P('tp'), may hold values from -4.5 to 1.5
- skip_gain: float32 [32], P('tp'), may hold values from 0.5 to 2
- group_gain: float32 [2048], P('tp'), may hold values from 0.1 to 1.9
- out_weight: bfloat16 [2048, 2048], P('tp', 'ep'), may hold values from -0.125 to 0.125
- second_gain: float32 [2048], replicated, may hold values from 0.1 to 1.9
- routes: int32 [256, 4], P('ep'), may hold values from 0 to 127, all different within a row; in each aligned block of 256 rows (0 to 255, 256 to 511, ...) at most 32 rows name the same one
- route_logits: bfloat16 [256, 4], P('ep'), may hold values from -8 to 300
- expert_gate: bfloat16 [128, 2048, 1024], P('ep', None, 'tp'), may hold values from -0.5 to 0.5
- expert_up: bfloat16 [128, 2048, 1024], P('ep', None, 'tp'), may hold values from -0.5 to 0.5
- expert_down: bfloat16 [128, 1024, 2048], P('ep', 'tp'), may hold values from -0.0234375 to 0.0234375
- dense_up: bfloat16 [2048, 4096], P(None, ('ep', 'tp')), may hold values from -0.125 to 0.125
- dense_down: bfloat16 [4096, 2048], P(('ep', 'tp')), may hold values from -0.09375 to 0.09375
- dense_gate: float32 [2048], replicated, may hold values from -0.125 to 0.125
Outputs:
- layer_out: bfloat16 [256, 2048], P(('ep', 'tp'))
- state_out: float32 [256, 32, 64, 128], P('ep', 'tp')
- conv_out: bfloat16 [256, 3, 2048], P('ep', None, 'tp')
- conv_proj_out: bfloat16 [256, 3, 2, 512], P('ep', None, None, 'tp')
Inputs may be any that keep to these rules, and one draw needn't show every extreme that they name: `routes`: each token names 4 different experts; over the whole batch no expert is named by more than 32 rows, a bound that some block reaches.
All inputs are finite; a program needn't handle non-finite values.
Results may differ from a plain program's by a relative error of at most 0.015.
Values may be sent and summed in bfloat16 or wider, within the bound.
No kernel may reach another device: no remote copies, remote signals or barrier semaphores. Data moves between devices by JAX's collectives and lax.ppermute only.
A program may use at most 64 MiB of HBM per device.

v0:
```python
import jax
import jax.numpy as jnp
from jax import lax
from jax.sharding import Mesh
from jax.sharding import PartitionSpec as P

GROUPS = 4
EP = ("ep_0", "ep_1", "ep_2")
EP_TP = ("ep_0", "ep_1", "ep_2", "tp")


norm_eps = 1e-05
clamp_limit = 7.0
glu_alpha = 1.702
highest = lax.Precision.HIGHEST


def in_one_piece(arrays, axis, dim, along):
    widths = [a.shape[along] for a in arrays]
    both = jnp.concatenate(arrays, axis=along)
    result = lax.all_gather(both, axis, axis=dim, tiled=True)
    return tuple(jnp.split(result, [sum(widths[:k]) for k in range(1, len(widths))], axis=along))


def gathered_by_axis(shard, axes, dim):
    if not axes:
        return shard
    nearer = lax.all_gather(shard, axes[-1], axis=dim, tiled=True)
    return gathered_by_axis(nearer, axes[:-1], dim)


def sent_to_all(shard, axis):
    copies = jnp.broadcast_to(shard, (lax.axis_size(axis), *shard.shape))
    return lax.all_to_all(copies, axis, split_axis=0, concat_axis=0, tiled=True)


def over_copies(shard, axis):
    everything = sent_to_all(shard, axis)
    return jnp.sum(everything, axis=0)


def rms_scale(values, gain_vec):
    return (
        values * lax.rsqrt(jnp.mean(values * values, axis=-1, keepdims=True) + norm_eps) * gain_vec
    )


def clamped_unit(gate_pre, up_pre):
    glu_part = jnp.minimum(gate_pre, clamp_limit)
    lin_part = jnp.clip(up_pre, -clamp_limit, clamp_limit)
    return glu_part * jax.nn.sigmoid(glu_alpha * glu_part) * (lin_part + 1.0)


def state_step(
    inner_proj,
    gate_proj,
    write_proj,
    read_proj,
    step_raw,
    conv_state,
    conv_proj_state,
    conv_kernel,
    conv_proj_kernel,
    step_bias,
    log_rate,
    skip_gain,
    group_gain,
    head_state,
    group_count,
):
    window_inner = jnp.concatenate([conv_state, inner_proj[:, None, :]], axis=1)
    window_proj = jnp.concatenate(
        [conv_proj_state, jnp.stack([write_proj, read_proj], axis=1)[:, None]], axis=1
    )
    conv_inner = jax.nn.silu(jnp.sum(window_inner.astype(jnp.float32) * conv_kernel[None], axis=1))
    conv_proj = jax.nn.silu(
        jnp.sum(window_proj.astype(jnp.float32) * conv_proj_kernel[None], axis=1)
    )
    seq_count, channels = conv_inner.shape
    head_count = step_raw.shape[1]
    head_width = channels // head_count
    state_width = conv_proj.shape[2] // group_count
    per_group = head_count // group_count
    head_input = conv_inner.reshape(seq_count, head_count, head_width)
    write_heads = jnp.repeat(
        conv_proj[:, 0].reshape(seq_count, group_count, state_width), per_group, axis=1
    )
    read_heads = jnp.repeat(
        conv_proj[:, 1].reshape(seq_count, group_count, state_width), per_group, axis=1
    )
    step_size = jax.nn.softplus(step_raw + step_bias)
    decay_rate = jnp.exp(-jnp.exp(log_rate) * step_size)
    state_out = (
        decay_rate[:, :, None, None] * head_state
        + (step_size[:, :, None] * head_input)[:, :, :, None] * write_heads[:, :, None, :]
    )
    read_out = (
        jnp.einsum("shpn,shn->shp", state_out, read_heads, precision=highest)
        + skip_gain[None, :, None] * head_input
    )
    gated_rows = read_out.reshape(seq_count, channels) * jax.nn.silu(gate_proj.astype(jnp.float32))
    grouped = gated_rows.reshape(seq_count, group_count, channels // group_count)
    grouped = grouped * lax.rsqrt(jnp.mean(grouped * grouped, axis=-1, keepdims=True) + norm_eps)
    mixer_rows = (grouped.reshape(seq_count, channels) * group_gain).astype(jnp.bfloat16)
    return (mixer_rows, state_out, window_inner[:, 1:], window_proj[:, 1:])


def local(
    tokens,
    head_state,
    conv_state,
    conv_proj_state,
    first_gain,
    gate_weight,
    inner_weight,
    write_weight,
    read_weight,
    step_weight,
    conv_kernel,
    conv_proj_kernel,
    step_bias,
    log_rate,
    skip_gain,
    group_gain,
    out_weight,
    second_gain,
    routes,
    route_logits,
    expert_gate,
    expert_up,
    expert_down,
    dense_up,
    dense_down,
    dense_gate,
):
    seq_count = tokens.shape[0]
    normed_in = rms_scale(tokens.astype(jnp.float32), first_gain).astype(jnp.bfloat16)
    pieces = in_one_piece((gate_weight, inner_weight), EP, 0, 1)
    gate_sum = jnp.dot(normed_in, pieces[0], preferred_element_type=jnp.float32)
    inner_sum = jnp.dot(normed_in, pieces[1], preferred_element_type=jnp.float32)
    gate_proj = gate_sum.astype(jnp.bfloat16)
    inner_proj = inner_sum.astype(jnp.bfloat16)
    write_proj = jnp.dot(normed_in, write_weight, preferred_element_type=jnp.float32).astype(
        jnp.bfloat16
    )
    read_proj = jnp.dot(normed_in, read_weight, preferred_element_type=jnp.float32).astype(
        jnp.bfloat16
    )
    step_raw = jnp.dot(normed_in, step_weight, preferred_element_type=jnp.float32)
    local_groups = GROUPS // lax.axis_size("tp")
    mixer_rows, state_out, conv_out, conv_proj_out = state_step(
        inner_proj,
        gate_proj,
        write_proj,
        read_proj,
        step_raw,
        conv_state,
        conv_proj_state,
        conv_kernel,
        conv_proj_kernel,
        step_bias,
        log_rate,
        skip_gain,
        group_gain,
        head_state,
        local_groups,
    )
    column_block = jnp.dot(
        gathered_by_axis(mixer_rows, EP, 0), out_weight, preferred_element_type=jnp.float32
    )
    partial_mix = lax.all_to_all(column_block, EP, split_axis=0, concat_axis=1, tiled=True)
    mixed = over_copies(partial_mix, "tp")
    hidden = (tokens.astype(jnp.float32) + mixed).astype(jnp.bfloat16)
    normed_mid = rms_scale(hidden.astype(jnp.float32), second_gain).astype(jnp.bfloat16)
    all_rows, all_routes, all_logits = (
        gathered_by_axis(normed_mid, EP, 0),
        gathered_by_axis(routes, EP, 0),
        gathered_by_axis(route_logits, EP, 0),
    )
    route_gates = jax.nn.softmax(all_logits.astype(jnp.float32), axis=-1)
    my_expert = lax.axis_index(EP)
    route_hits = all_routes == my_expert
    row_weight = jnp.sum(jnp.where(route_hits, route_gates, 0.0), axis=1)
    chosen = jnp.any(route_hits, axis=1)
    slot_index = jnp.cumsum(chosen.astype(jnp.int32)) - 1
    capacity = 4 * seq_count * routes.shape[1]
    slot_ids = jnp.arange(capacity, dtype=jnp.int32)
    picks = (slot_index[None, :] == slot_ids[:, None]) & chosen[None, :]
    picked_rows = jnp.dot(
        picks.astype(jnp.bfloat16), all_rows, preferred_element_type=jnp.float32
    ).astype(jnp.bfloat16)
    activated = clamped_unit(
        jnp.dot(picked_rows, expert_gate[0], preferred_element_type=jnp.float32),
        jnp.dot(picked_rows, expert_up[0], preferred_element_type=jnp.float32),
    ).astype(jnp.bfloat16)
    expert_part = jnp.dot(activated, expert_down[0], preferred_element_type=jnp.float32)
    placed = jnp.where(picks, row_weight[None, :], 0.0)
    dense_weight = jax.nn.sigmoid(
        jnp.dot(all_rows.astype(jnp.float32), dense_gate, precision=highest)
    )
    row_share = seq_count // lax.axis_size("tp")
    down_half = lax.all_to_all(dense_down, "tp", split_axis=1, concat_axis=0, tiled=True)
    dense_inner = jax.nn.silu(
        jnp.dot(all_rows, dense_up, preferred_element_type=jnp.float32)
    ).astype(jnp.bfloat16)
    pair_inner = lax.all_gather(dense_inner, "tp", axis=1, tiled=True)
    expert_cols = lax.psum_scatter(
        expert_part.astype(jnp.bfloat16), "tp", scatter_dimension=1, tiled=True
    ).astype(jnp.float32)
    dense_term = (
        jnp.dot(pair_inner, down_half, preferred_element_type=jnp.float32) * dense_weight[:, None]
    )
    column_sums = lax.psum_scatter(
        dense_term + jnp.einsum("cr,cd->rd", placed, expert_cols, precision=highest),
        EP,
        scatter_dimension=0,
        tiled=True,
    )
    summed = lax.all_to_all(column_sums, "tp", split_axis=0, concat_axis=1, tiled=True)
    own_rows = lax.dynamic_slice_in_dim(hidden, lax.axis_index("tp") * row_share, row_share, 0)
    layer_out = (own_rows.astype(jnp.float32) + summed).astype(jnp.bfloat16)
    return (layer_out, state_out, conv_out, conv_proj_out)


def solution(mesh):
    torus = Mesh(mesh.devices.reshape(8, 4, 4, mesh.shape["tp"]), ("ep_0", "ep_1", "ep_2", "tp"))
    return jax.shard_map(
        local,
        mesh=torus,
        in_specs=(
            P(EP, None),
            P(EP, "tp", None, None),
            P(EP, None, "tp"),
            P(EP, None, None, "tp"),
            P(),
            P(EP, "tp"),
            P(EP, "tp"),
            P(None, "tp"),
            P(None, "tp"),
            P(None, "tp"),
            P(None, "tp"),
            P(None, None, "tp"),
            P("tp"),
            P("tp"),
            P("tp"),
            P("tp"),
            P("tp", EP),
            P(),
            P(EP, None),
            P(EP, None),
            P(EP, None, "tp"),
            P(EP, None, "tp"),
            P(EP, "tp", None),
            P(None, EP_TP),
            P(EP_TP, None),
            P(),
        ),
        out_specs=(
            P(EP_TP, None),
            P(EP, "tp", None, None),
            P(EP, None, "tp"),
            P(EP, None, None, "tp"),
        ),
        check_vma=False,
    )
```

profile of v0, /device:TPU:1, one launch (start us, length us, event | category | flops | bytes accessed | tf_op | source)
XLA Modules:
  0.0 581.7 jit_solution(3944706384839282891)
XLA Ops:
  7.3 1.5 pad_maximum_fusion
  8.9 0.8 fusion.57
  9.8 1.5 fusion.38
  11.3 1.5 fusion.39
  13.3 123.4 %all-gather.11.cloned.1.call-done = bf16[2048,2048]{1,0:T(8,128)(2,1)} async-done(((bf16[16,2048]{1,0:T(8,128)(2,1)}), bf16[2048,2048]{1,0:T(8,128)(2,1)}) %all-gather.11.cloned.1.call-update) | async-done | bytes 8388624 | tf_op jit(solution)/shard_map/all_gather | solution.py:21
  136.7 2.9 fusion.35
  140.2 0.9 copy-done.2
  141.1 1.7 fusion.89
  143.0 2.9 fusion.88
  146.2 9.4 %all-gather = bf16[4,2,1024]{2,1,0:T(2,128)(2,1)S(1)} all-gather(bf16[1,2,1024]{2,1,0:T(2,128)(2,1)S(1)} %fusion.72), channel_id=1, replica_groups=mesh['ep_0'=8,'ep_1'=4,'ep_2'=4,'tp'=2] {'ep_2'}, dimensions={0}, use_global_device_ids=true | all-gather | bytes 20480 | tf_op jit(solution)/shard_map/all_gather | solution.py:28
  155.7 9.0 %all_gather.44 = bf16[32,1024]{1,0:T(8,128)(2,1)S(1)} all-gather(bf16[8,1024]{1,0:T(8,128)(2,1)S(1)} %reshape.119), channel_id=1, replica_groups=mesh['ep_0'=8,'ep_1'=4,'ep_2'=4,'tp'=2] {'ep_1'}, dimensions={0}, use_global_device_ids=true | all-gather | bytes 81920 | tf_op jit(solution)/shard_map/all_gather | solution.py:28
  164.7 20.8 %all_gather.45 = bf16[256,1024]{1,0:T(8,128)(2,1)S(1)} all-gather(bf16[32,1024]{1,0:T(8,128)(2,1)S(1)} %all_gather.44), channel_id=1, replica_groups=mesh['ep_0'=8,'ep_1'=4,'ep_2'=4,'tp'=2] {'ep_0'}, dimensions={0}, use_global_device_ids=true | all-gather | bytes 589824 | tf_op jit(solution)/shard_map/all_gather | solution.py:28
  185.7 19.8 %all_to_all.59 = f32[128,2,16]{2,1,0:T(2,128)S(1)} all-to-all(f32[128,2,16]{2,1,0:T(2,128)S(1)} %bitcast.96), channel_id=1, replica_groups=mesh['ep_0'=8,'ep_1'=4,'ep_2'=4,'tp'=2] {'ep_0','ep_1','ep_2'}, dimensions={0} | all-to-all | bytes 32768 | tf_op jit(solution)/shard_map/all_to_all | solution.py:171
  205.6 20.4 %all_to_all.60 = f32[2,2,2048]{2,1,0:T(2,128)S(1)} all-to-all(f32[2,2,2048]{2,1,0:T(2,128)S(1)} %broadcast_in_dim.26), channel_id=1, replica_groups=mesh['ep_0'=8,'ep_1'=4,'ep_2'=4,'tp'=2] {'tp'}, dimensions={0} | all-to-all | bytes 65536 | tf_op jit(solution)/shard_map/all_to_all | solution.py:34
  226.3 9.0 %all-gather.1 = bf16[4,2,2048]{2,1,0:T(2,128)(2,1)S(1)} all-gather(bf16[1,2,2048]{2,1,0:T(2,128)(2,1)S(1)} %fusion.71), channel_id=1, replica_groups=mesh['ep_0'=8,'ep_1'=4,'ep_2'=4,'tp'=2] {'ep_2'}, dimensions={0}, use_global_device_ids=true | all-gather | bytes 40960 | tf_op jit(solution)/shard_map/all_gather | solution.py:28
  235.3 10.3 %all_gather.47 = bf16[32,2048]{1,0:T(8,128)(2,1)} all-gather(bf16[8,2048]{1,0:T(8,128)(2,1)S(1)} %reshape.121), channel_id=1, replica_groups=mesh['ep_0'=8,'ep_1'=4,'ep_2'=4,'tp'=2] {'ep_1'}, dimensions={0}, use_global_device_ids=true | all-gather | bytes 163840 | tf_op jit(solution)/shard_map/all_gather | solution.py:28
  246.3 8.9 %all-to-all-start.2 = ((bf16[16,2,1024]{2,0,1:T(8,128)(2,1)}), bf16[16,2,1024]{2,0,1:T(8,128)(2,1)S(1)}, u32[]{:S(2)}, u32[]{:S(2)}) async-start(bf16[16,2,1024]{2,0,1:T(8,128)(2,1)} %bitcast.94), calls=%async_computation.2 | async-start | bytes 131072 | tf_op jit(solution)/shard_map/all_to_all | solution.py:202
  255.2 5.8 %all-gather.5 = bf16[4,2,4]{2,1,0:T(2,128)(2,1)S(1)} all-gather(bf16[1,2,4]{2,1,0:T(2,128)(2,1)S(1)} %bitcast.110), channel_id=1, replica_groups=mesh['ep_0'=8,'ep_1'=4,'ep_2'=4,'tp'=2] {'ep_2'}, dimensions={0}, use_global_device_ids=true | all-gather | bytes 80 | tf_op jit(solution)/shard_map/all_gather | solution.py:28
  261.1 7.1 %all-gather.2 = s32[4,2,4]{2,1,0:T(2,128)S(1)} all-gather(s32[1,2,4]{2,1,0:T(2,128)S(1)} %bitcast.109), channel_id=1, replica_groups=mesh['ep_0'=8,'ep_1'=4,'ep_2'=4,'tp'=2] {'ep_2'}, dimensions={0}, use_global_device_ids=true | all-gather | bytes 160 | tf_op jit(solution)/shard_map/all_gather | solution.py:28
  268.3 8.6 %all-gather.3 = s32[4,8,4]{1,2,0:T(4,128)S(1)} all-gather(s32[1,8,4]{1,2,0:T(4,128)S(1)} %copy.74), channel_id=1, replica_groups=mesh['ep_0'=8,'ep_1'=4,'ep_2'=4,'tp'=2] {'ep_1'}, dimensions={0}, use_global_device_ids=true | all-gather | bytes 640 | tf_op jit(solution)/shard_map/all_gather | solution.py:28
  277.0 16.0 %all-gather.4 = s32[8,32,4]{1,2,0:T(4,128)S(1)} all-gather(s32[1,32,4]{1,2,0:T(4,128)S(1)} %reshape.126), channel_id=1, replica_groups=mesh['ep_0'=8,'ep_1'=4,'ep_2'=4,'tp'=2] {'ep_0'}, dimensions={0}, use_global_device_ids=true | all-gather | bytes 4608 | tf_op jit(solution)/shard_map/all_gather | solution.py:28
  293.7 5.3 all-gather.6
  299.2 9.8 %all-gather.7 = bf16[8,32,4]{1,2,0:T(4,128)(2,1)S(1)} all-gather(bf16[1,32,4]{1,2,0:T(4,128)(2,1)S(1)} %reshape.132), channel_id=1, replica_groups=mesh['ep_0'=8,'ep_1'=4,'ep_2'=4,'tp'=2] {'ep_0'}, dimensions={0}, use_global_device_ids=true | all-gather | bytes 2304 | tf_op jit(solution)/shard_map/all_gather | solution.py:28
  309.4 1.5 convolution_convert_fusion.1
  310.9 2.0 fusion.9
  313.0 3.2 convolution_convert_fusion
  316.8 0.9 fusion.91
  317.7 17.9 %all_gather.49 = bf16[256,32]{0,1:T(8,128)(2,1)S(1)} all-gather(bf16[256,16]{0,1:T(8,128)(2,1)S(1)} %multiply_convert_fusion), channel_id=1, replica_groups=mesh['ep_0'=8,'ep_1'=4,'ep_2'=4,'tp'=2] {'tp'}, dimensions={1}, use_global_device_ids=true | all-gather | bytes 24576 | tf_op jit(solution)/shard_map/all_gather | solution.py:206
  336.0 4.8 reduce-scatter.2.cloned.1.call-done
  340.8 2.5 convolution_add_fusion
  345.7 219.4 %all-reduce.3.cloned.1.call-done = f32[256,1024]{1,0:T(8,128)} async-done(((f32[256,1024]{1,0:T(8,128)}), f32[256,1024]{1,0:T(8,128)}) %all-reduce.3.cloned.1.call-update) | async-done | bytes 1048592
  565.9 8.7 %all_to_all.61 = f32[2,1,1024]{2,1,0:T(1,128)S(1)} all-to-all(f32[2,1,1024]{2,1,0:T(1,128)S(1)} %copy.80), channel_id=1, replica_groups=mesh['ep_0'=8,'ep_1'=4,'ep_2'=4,'tp'=2] {'tp'}, dimensions={0} | all-to-all | bytes 16384 | tf_op jit(solution)/shard_map/all_to_all | solution.py:219
  (120 shorter events, 8.2 us)
Async XLA Ops:
  7.2 305.8 %copy-start = (bf16[1,512,2048]{2,1,0:T(8,128)(2,1)S(1)}, bf16[1,512,2048]{2,1,0:T(8,128)(2,1)}, u32[]{:S(2)}) copy-start(bf16[1,512,2048]{2,1,0:T(8,128)(2,1)} %param.48) | copy-start | bytes 6291460
  7.2 5.8 %copy-start.4 = (bf16[2,2048]{1,0:T(2,128)(2,1)S(1)}, bf16[2,2048]{1,0:T(2,128)(2,1)}, u32[]{:S(2)}) copy-start(bf16[2,2048]{1,0:T(2,128)(2,1)} %param.26) | copy-start | bytes 24580
  7.2 5.8 %copy-start.5 = (f32[2048]{0:T(1024)S(1)}, f32[2048]{0:T(1024)}, u32[]{:S(2)}) copy-start(f32[2048]{0:T(1024)} %param.30) | copy-start | bytes 24580
  7.2 5.7 copy-start.14
  7.2 5.7 copy-start.13
  7.2 5.7 copy-start.20
  7.2 5.8 copy-start.19
  7.2 5.8 copy-start.21
  7.3 129.4 %all-gather.11.cloned.1.call-start = ((), (), s32[]{:S(2)}) async-start(), calls=%async_computation.5 | async-start | bytes 8454144 | tf_op jit(solution)/shard_map/all_gather | solution.py:21
  8.9 300.6 %all-gather.13.cloned.1.call-start = ((), (), s32[]{:S(2)}) async-start(), calls=%async_computation.6 | async-start | bytes 1179648 | tf_op jit(solution)/shard_map/all_gather | solution.py:28
  13.3 126.3 %copy-start.8 = (bf16[2,3,1024]{2,0,1:T(2,128)(2,1)S(1)}, bf16[2,3,1024]{2,0,1:T(2,128)(2,1)}, u32[]{:S(2)}) copy-start(bf16[2,3,1024]{2,0,1:T(2,128)(2,1)} %param.28) | copy-start | bytes 36868
  13.3 126.3 %copy-start.10 = (f32[4,1024]{1,0:T(4,128)S(1)}, f32[4,1024]{1,0:T(4,128)}, u32[]{:S(2)}) copy-start(f32[4,1024]{1,0:T(4,128)} %param.36) | copy-start | bytes 49156
  13.3 126.5 %copy-start.3 = (f32[2,16,64,128]{3,2,1,0:T(8,128)S(1)}, f32[2,16,64,128]{3,2,1,0:T(8,128)}, u32[]{:S(2)}) copy-start(f32[2,16,64,128]{3,2,1,0:T(8,128)} %param.27) | copy-start | bytes 3145732
  139.5 3.3 copy-start.17
  140.1 1.0 copy-start.2
  143.0 3.2 copy-start.15
  143.0 42.4 %copy-start.9 = (bf16[1024,16]{0,1:T(8,128)(2,1)S(1)}, bf16[1024,16]{0,1:T(8,128)(2,1)}, u32[]{:S(2)}) copy-start(bf16[1024,16]{0,1:T(8,128)(2,1)} %param.42) | copy-start | bytes 98308
  145.9 80.2 %copy-start.12 = (f32[2048]{0:T(1024)S(1)}, f32[2048]{0:T(1024)}, u32[]{:S(2)}) copy-start(f32[2048]{0:T(1024)} %param.43) | copy-start | bytes 24580
  145.9 99.7 %copy-start.7 = (bf16[16,2048]{1,0:T(8,128)(2,1)S(1)}, bf16[16,2048]{1,0:T(8,128)(2,1)}, u32[]{:S(2)}) copy-start(bf16[16,2048]{1,0:T(8,128)(2,1)} %param.50) | copy-start | bytes 196612
  146.0 109.3 %copy-start.18 = (bf16[2,4]{1,0:T(2,128)(2,1)S(1)}, bf16[2,4]{1,0:T(2,128)(2,1)}, u32[]{:S(2)}) copy-start(bf16[2,4]{1,0:T(2,128)(2,1)} %param.45) | copy-start | bytes 52
  146.0 115.1 %copy-start.16 = (s32[2,4]{1,0:T(2,128)S(1)}, s32[2,4]{1,0:T(2,128)}, u32[]{:S(2)}) copy-start(s32[2,4]{1,0:T(2,128)} %param.44) | copy-start | bytes 100
  246.3 89.4 %all-to-all-start.2 = ((bf16[16,2,1024]{2,0,1:T(8,128)(2,1)}), bf16[16,2,1024]{2,0,1:T(8,128)(2,1)S(1)}, u32[]{:S(2)}, u32[]{:S(2)}) async-start(bf16[16,2,1024]{2,0,1:T(8,128)(2,1)} %bitcast.94), calls=%async_computation.2 | async-start | bytes 131072 | tf_op jit(solution)/shard_map/all_to_all | solution.py:202
  255.2 85.6 %reduce-scatter.2.cloned.1.call-start = ((), (), s32[]{:S(2)}) async-start(), calls=%async_computation.7 | async-start | bytes 196608 | tf_op jit(solution)/shard_map/reduce_scatter | solution.py:207
  313.0 3.3 copy-start.1
  313.0 3.3 copy-start.6
  313.0 3.7 copy-start.11
  316.3 248.9 %all-reduce.3.cloned.1.call-start = ((), (), s32[]{:S(2)}) async-start(), calls=%async_computation.8 | async-start | bytes 2097152
  335.7 8.2 %copy-start.22 = (u32[256]{0:T(256)S(1)}, u32[256]{0:T(256)}, u32[]{:S(2)}) copy-start(u32[256]{0:T(256)} %constant.83) | copy-start | bytes 3076
Sparse Core Ops, SparseCore 0:
  12.3 124.3 all-gather.10
  245.8 32.3 all-gather.12
  316.4 24.3 reduce-scatter.1
  346.0 219.1 all-reduce.2
where the time goes:
time: 583 us; the launch traced here: 582 us
  waiting for transfers between devices  348 us (60%)
  blocking collectives  178 us (31%)
  matrix products  21.9 us (4%)
  between operations  14.9 us (3%)
  starting transfers between devices  9.06 us (2%)
    unnamed x5, waiting for transfers between devices  219 us
    all_gather x1, waiting for transfers between devices, in_one_piece(): result = lax.all_gather(both, axis, axis=dim, tiled=True)  123 us
    all_gather x11, blocking collectives, gathered_by_axis(): nearer = lax.all_gather(shard, axes[-1], axis=dim, tiled=True)  111 us
    all_to_all x1, blocking collectives, sent_to_all(): return lax.all_to_all(copies, axis, split_axis=0, concat_axis=0, tiled=True)  20.4 us
    all_to_all x1, blocking collectives, local(): lax.all_to_all(column_block, EP, split_axis=0, concat_axis=1, tiled=True)  19.8 us
    all_gather x1, blocking collectives, local(): pair_inner = lax.all_gather(dense_inner, 'tp', axis=1, tiled=True)  17.9 us
  transfers between devices with their start and end apart: 5, of which 3 were waited for; matrix products, arithmetic and copies ran while one was open for 3% of the time, Pallas kernels for 0%

commit v1 on v0

v1 whole, which is shorter than its diff:
```python
import jax
import jax.numpy as jnp
from jax import lax
from jax.sharding import Mesh
from jax.sharding import PartitionSpec as P

GROUPS = 4
ROW_AXES = ("z", "y")
ROW_TP = ("z", "y", "tp")
EP = ("z", "y", "x")
EP_TP = ("z", "y", "x", "tp")


norm_eps = 1e-05
clamp_limit = 7.0
glu_alpha = 1.702
highest = lax.Precision.HIGHEST
f32 = jnp.float32
bf16 = jnp.bfloat16


def exchanged(pieces, axis):
    return lax.all_to_all(pieces, axis, split_axis=0, concat_axis=0, tiled=True)


def shifted(block, axis, by):
    size = lax.axis_size(axis)
    return lax.ppermute(block, axis, [(i, (i + by) % size) for i in range(size)])


def rms_scale(values, gain_vec):
    return (
        values * lax.rsqrt(jnp.mean(values * values, axis=-1, keepdims=True) + norm_eps) * gain_vec
    )


def clamped_unit(gate_pre, up_pre):
    glu_part = jnp.minimum(gate_pre, clamp_limit)
    lin_part = jnp.clip(up_pre, -clamp_limit, clamp_limit)
    return glu_part * jax.nn.sigmoid(glu_alpha * glu_part) * (lin_part + 1.0)


def state_step(
    inner_proj,
    gate_proj,
    write_proj,
    read_proj,
    step_raw,
    conv_state,
    conv_proj_state,
    conv_kernel,
    conv_proj_kernel,
    step_bias,
    log_rate,
    skip_gain,
    group_gain,
    head_state,
    group_count,
):
    window_inner = jnp.concatenate([conv_state, inner_proj[:, None, :]], axis=1)
    window_proj = jnp.concatenate(
        [conv_proj_state, jnp.stack([write_proj, read_proj], axis=1)[:, None]], axis=1
    )
    conv_inner = jax.nn.silu(jnp.sum(window_inner.astype(f32) * conv_kernel[None], axis=1))
    conv_proj = jax.nn.silu(jnp.sum(window_proj.astype(f32) * conv_proj_kernel[None], axis=1))
    seq_count, channels = conv_inner.shape
    head_count = step_raw.shape[1]
    head_width = channels // head_count
    state_width = conv_proj.shape[2] // group_count
    per_group = head_count // group_count
    head_input = conv_inner.reshape(seq_count, head_count, head_width)
    write_heads = jnp.repeat(
        conv_proj[:, 0].reshape(seq_count, group_count, state_width), per_group, axis=1
    )
    read_heads = jnp.repeat(
        conv_proj[:, 1].reshape(seq_count, group_count, state_width), per_group, axis=1
    )
    step_size = jax.nn.softplus(step_raw + step_bias)
    decay_rate = jnp.exp(-jnp.exp(log_rate) * step_size)
    state_out = (
        decay_rate[:, :, None, None] * head_state
        + (step_size[:, :, None] * head_input)[:, :, :, None] * write_heads[:, :, None, :]
    )
    read_out = (
        jnp.sum(state_out * read_heads[:, :, None, :], axis=-1)
        + skip_gain[None, :, None] * head_input
    )
    gated_rows = read_out.reshape(seq_count, channels) * jax.nn.silu(gate_proj.astype(f32))
    grouped = gated_rows.reshape(seq_count, group_count, channels // group_count)
    grouped = grouped * lax.rsqrt(jnp.mean(grouped * grouped, axis=-1, keepdims=True) + norm_eps)
    mixer_rows = (grouped.reshape(seq_count, channels) * group_gain).astype(bf16)
    return (mixer_rows, state_out, window_inner[:, 1:], window_proj[:, 1:])


def local(
    tokens,
    head_state,
    conv_state,
    conv_proj_state,
    first_gain,
    gate_weight,
    inner_weight,
    write_weight,
    read_weight,
    step_weight,
    conv_kernel,
    conv_proj_kernel,
    step_bias,
    log_rate,
    skip_gain,
    group_gain,
    out_weight,
    second_gain,
    routes,
    route_logits,
    expert_gate,
    expert_up,
    expert_down,
    dense_up,
    dense_down,
    dense_gate,
):
    seq_count, width = tokens.shape
    topk = routes.shape[1]
    capacity = 4 * seq_count * topk
    rows_n = lax.axis_size(ROW_AXES)
    line_n = lax.axis_size("x")
    row_at = lax.axis_index(ROW_AXES)
    line_at = lax.axis_index("x")
    tp_at = lax.axis_index("tp")
    share = gate_weight.shape[0]
    block = share * line_n
    batch = rows_n * seq_count
    channels = gate_weight.shape[1]

    normed_in = rms_scale(tokens.astype(f32), first_gain).astype(bf16)
    features = jnp.concatenate(
        [
            tokens.reshape(seq_count, rows_n, block),
            normed_in.reshape(seq_count, rows_n, block),
            jnp.broadcast_to(routes.astype(bf16)[:, None], (seq_count, rows_n, topk)),
            jnp.broadcast_to(route_logits[:, None], (seq_count, rows_n, topk)),
        ],
        axis=2,
    )
    with jax.named_scope("spread_tokens"):
        spread = exchanged(jnp.transpose(features, (1, 0, 2)), ROW_AXES)
    spread = spread.reshape(batch, 2 * block + 2 * topk)
    raw_block = spread[:, :block]
    normed_block = spread[:, block : 2 * block]
    all_routes = spread[:, 2 * block : 2 * block + topk]
    all_logits = spread[:, 2 * block + topk :].astype(f32)

    with jax.named_scope("line_weights"):
        held = jnp.concatenate(
            [
                jnp.concatenate([gate_weight, inner_weight], axis=1),
                dense_down,
                dense_up.T,
                out_weight.T.reshape(share // 2, 2 * channels),
            ],
            axis=0,
        )
        lines = jnp.stack([held] + [shifted(held, "x", -by) for by in range(1, line_n)])
    order = jnp.arange(block, dtype=jnp.int32)
    unturn = ((order[:, None] - share * line_at) % block == order[None, :]).astype(bf16)

    def natural(part):
        return jnp.dot(unturn, part, preferred_element_type=f32).astype(bf16)

    in_weight = natural(lines[:, :share].reshape(block, 2 * channels))
    line_down = lines[:, share : 2 * share].reshape(block, width)
    line_up = lines[:, 2 * share : 3 * share].reshape(block, width)
    line_out = natural(lines[:, 3 * share :].reshape(block, channels))

    with jax.named_scope("in_proj"):
        in_part = jnp.dot(normed_block, in_weight, preferred_element_type=f32).astype(bf16)
        in_terms = exchanged(in_part.reshape(rows_n, seq_count, 2 * channels), ROW_AXES)
        in_sum = jnp.sum(in_terms.astype(f32), axis=0).astype(bf16)
    gate_proj, inner_proj = in_sum[:, :channels], in_sum[:, channels:]
    write_proj = jnp.dot(normed_in, write_weight, preferred_element_type=f32).astype(bf16)
    read_proj = jnp.dot(normed_in, read_weight, preferred_element_type=f32).astype(bf16)
    step_raw = jnp.dot(normed_in, step_weight, preferred_element_type=f32)
    with jax.named_scope("state"):
        mixer_rows, state_out, conv_out, conv_proj_out = state_step(
            inner_proj,
            gate_proj,
            write_proj,
            read_proj,
            step_raw,
            conv_state,
            conv_proj_state,
            conv_kernel,
            conv_proj_kernel,
            step_bias,
            log_rate,
            skip_gain,
            group_gain,
            head_state,
            GROUPS // lax.axis_size("tp"),
        )
    with jax.named_scope("out_proj"):
        mixer_all = exchanged(
            jnp.broadcast_to(mixer_rows, (rows_n, seq_count, channels)), ROW_AXES
        ).reshape(batch, channels)
        mixed_part = lax.dot_general(
            line_out, mixer_all, (((1,), (1,)), ((), ())), preferred_element_type=f32
        )
        mixed = mixed_part + shifted(mixed_part, "tp", 1)
        hidden_block = (raw_block.T.astype(f32) + mixed).astype(bf16)
    with jax.named_scope("hidden"):
        hidden = exchanged(
            jnp.broadcast_to(hidden_block, (rows_n, block, batch)), ROW_AXES
        ).reshape(width, batch)
        hidden_wide = hidden.astype(f32)
        normed_mid = (
            hidden_wide
            * lax.rsqrt(jnp.mean(hidden_wide * hidden_wide, axis=0, keepdims=True) + norm_eps)
            * second_gain[:, None]
        ).astype(bf16)

    route_gates = jax.nn.softmax(all_logits, axis=-1)
    experts = (line_n * row_at + (line_at + jnp.arange(line_n)) % line_n).astype(bf16)
    hits = all_routes[None] == experts[:, None, None]
    row_weight = jnp.sum(jnp.where(hits, route_gates[None], 0.0), axis=2)
    chosen = jnp.any(hits, axis=2)
    earlier = (jnp.arange(batch)[:, None] < jnp.arange(batch)[None, :]).astype(bf16)
    slot = jnp.dot(chosen.astype(bf16), earlier, preferred_element_type=f32)
    slot_ids = jnp.arange(capacity, dtype=f32)
    picks = (slot[:, None, :] == slot_ids[None, :, None]) & chosen[:, None, :]
    placed = jnp.where(picks, row_weight[:, None, :], 0.0).astype(bf16)
    picks = picks.astype(bf16).reshape(line_n * capacity, batch)
    placed = placed.reshape(line_n * capacity, batch)

    with jax.named_scope("dispatch"):
        sent = lax.dot_general(
            picks, normed_mid, (((1,), (1,)), ((), ())), preferred_element_type=f32
        ).astype(bf16)
        sent = sent.reshape(line_n, capacity, width)
        rows = jnp.concatenate(
            [sent[0]] + [shifted(sent[by], "x", by) for by in range(1, line_n)], axis=0
        )
    with jax.named_scope("expert"):
        activated = clamped_unit(
            jnp.dot(rows, expert_gate[0], preferred_element_type=f32),
            jnp.dot(rows, expert_up[0], preferred_element_type=f32),
        ).astype(bf16)
        expert_rows = jnp.dot(activated, expert_down[0], preferred_element_type=f32).astype(bf16)
        expert_rows = expert_rows.reshape(line_n, capacity, width)
        returned = jnp.concatenate(
            [expert_rows[0]]
            + [shifted(expert_rows[by], "x", -by) for by in range(1, line_n)],
            axis=0,
        )
    with jax.named_scope("dense"):
        dense_weight = jax.nn.sigmoid(
            jnp.sum(normed_mid.astype(f32) * dense_gate[:, None], axis=0)
        )
        dense_inner = jax.nn.silu(
            jnp.dot(line_up, normed_mid, preferred_element_type=f32)
        ).astype(bf16)
        dense_term = (
            lax.dot_general(
                dense_inner, line_down, (((0,), (0,)), ((), ())), preferred_element_type=f32
            )
            * dense_weight[:, None]
        )
    with jax.named_scope("combine"):
        expert_term = lax.dot_general(
            placed, returned, (((0,), (0,)), ((), ())), preferred_element_type=f32
        )
        terms = (dense_term + expert_term).astype(bf16)
        terms = exchanged(terms.reshape(batch, 1, width), ROW_TP)
        own = (jnp.arange(batch) == seq_count * row_at + tp_at).astype(bf16)
        own_row = lax.dot_general(
            jnp.broadcast_to(own, (8, batch)),
            hidden,
            (((1,), (1,)), ((), ())),
            preferred_element_type=f32,
        )[:1]
        layer_out = (own_row + jnp.sum(terms.astype(f32), axis=0)).astype(bf16)
    return (layer_out, state_out, conv_out, conv_proj_out)


def solution(mesh):
    torus = Mesh(mesh.devices.reshape(8, 4, 4, mesh.shape["tp"]), EP_TP)
    return jax.shard_map(
        local,
        mesh=torus,
        in_specs=(
            P(EP, None),
            P(EP, "tp", None, None),
            P(EP, None, "tp"),
            P(EP, None, None, "tp"),
            P(),
            P(EP, "tp"),
            P(EP, "tp"),
            P(None, "tp"),
            P(None, "tp"),
            P(None, "tp"),
            P(None, "tp"),
            P(None, None, "tp"),
            P("tp"),
            P("tp"),
            P("tp"),
            P("tp"),
            P("tp", EP),
            P(),
            P(EP, None),
            P(EP, None),
            P(EP, None, "tp"),
            P(EP, None, "tp"),
            P(EP, "tp", None),
            P(None, EP_TP),
            P(EP_TP, None),
            P(),
        ),
        out_specs=(
            P(EP_TP, None),
            P(EP, "tp", None, None),
            P(EP, None, "tp"),
            P(EP, None, None, "tp"),
        ),
        check_vma=False,
    )
```

time: 583 us -> 145 us (0.25)
  waiting for transfers between devices: 348 us -> 54.6 us
  blocking collectives: 178 us -> 0 us
  starting transfers between devices: 9.06 us -> 48.6 us
  between operations: 14.9 us -> 1.1 us
  other arithmetic: 5.14 us -> 15.5 us
  matrix products: 21.9 us -> 12.2 us
  local copies, waits for them, and re-layouts: 5.03 us -> 12.3 us
    unnamed x5 -> x0, waiting for transfers between devices: 219 us -> none
    all_gather x12 -> x0, blocking collectives: 129 us -> none  [the longest x11 111 us: gathered_by_axis(): nearer = lax.all_gather(shard, axes[-1], axis=dim, tiled=True)]
    all_gather x2 -> x0, waiting for transfers between devices: 123 us -> none  [the longest x1 123 us: in_one_piece(): result = lax.all_gather(both, axis, axis=dim, tiled=True)]
    all_to_all x3 -> x0, blocking collectives: 48.8 us -> none  [the longest x1 20.4 us: sent_to_all(): return lax.all_to_all(copies, axis, split_axis=0, concat_axis=0, tiled=True)]
    all_to_all x1 -> x5, waiting for transfers between devices: 0.01 us -> 45.8 us  [exchanged(): return lax.all_to_all(pieces, axis, split_axis=0, concat_axis=0, tiled=True)]
    all_to_all x1 -> x5, starting transfers between devices: 8.94 us -> 33.2 us  [exchanged(): return lax.all_to_all(pieces, axis, split_axis=0, concat_axis=0, tiled=True)]
    ppermute x0 -> x10, starting transfers between devices: none -> 15.4 us  [shifted(): lax.ppermute(block, axis, [(i, (i + by) % size) for i in range(size)])]
    dot_general x14 -> x12, matrix products: 21.9 us -> 12.2 us  [the longest x1 3.4 us: local(): jnp.dot(activated, expert_down[0], preferred_element_type=f32).astype(bf16)]
  transfers between devices with their start and end apart: 5 -> 15, of which waited for: 3 -> 11; matrix products, arithmetic and copies ran while one was open for 3% -> 10% of each run, Pallas kernels for 0% -> 0%
where the time goes in v1:
time: 145 us; the launch traced here: 144 us
  waiting for transfers between devices  54.6 us (38%)
  starting transfers between devices  48.6 us (34%)
  other arithmetic  15.5 us (11%)
  local copies, waits for them, and re-layouts  12.3 us (8%)
  matrix products  12.2 us (8%)
    all_to_all x5, waiting for transfers between devices, exchanged(): return lax.all_to_all(pieces, axis, split_axis=0, concat_axis=0, tiled=True)  45.8 us
    all_to_all x5, starting transfers between devices, exchanged(): return lax.all_to_all(pieces, axis, split_axis=0, concat_axis=0, tiled=True)  33.2 us
    ppermute x10, starting transfers between devices, shifted(): lax.ppermute(block, axis, [(i, (i + by) % size) for i in range(size)])  15.4 us
    ppermute x10, waiting for transfers between devices, shifted(): lax.ppermute(block, axis, [(i, (i + by) % size) for i in range(size)])  8.76 us
    unnamed x43, local copies, waits for them, and re-layouts  4.23 us
    dot_general x1, matrix products, local(): jnp.dot(activated, expert_down[0], preferred_element_type=f32).astype(bf16)  3.4 us
  transfers between devices with their start and end apart: 15, of which 11 were waited for; matrix products, arithmetic and copies ran while one was open for 10% of the time, Pallas kernels for 0%

profile of v1, /device:TPU:1, one launch (start us, length us, event | category | flops | bytes accessed | tf_op | source)
XLA Modules:
  0.0 144.3 jit_solution(17216555563013658142)
XLA Ops:
  0.7 0.9 reshape.260
  1.6 1.6 %pad_maximum_fusion.6 = bf16[56,2048]{1,0:T(8,128)(2,1)} fusion(bf16[8,2048]{1,0:T(8,128)(2,1)S(1)} %reshape.260, bf16[16,2048]{1,0:T(8,128)(2,1)} %bitcast.96, bf16[16,2048]{1,0:T(8,128)(2,1)} %param.50, bf16[16,1024]{1,0:T(8,128)(2,1)} %param.32, bf16[16,1024]{1,0:T(8,128)(2,1)} %param.31), kind=kLoop, calls=%fused_computation.48 | loop fusion | flops 1146880 | bytes 458752 | tf_op jit(solution)/shard_map/line_weights/concatenate | solution.py:155
  3.3 2.0 %collective-permute-start.2 = (bf16[56,2048]{1,0:T(8,128)(2,1)}, bf16[56,2048]{1,0:T(8,128)(2,1)}, u32[]{:S(2)}, u32[]{:S(2)}) collective-permute-start(bf16[56,2048]{1,0:T(8,128)(2,1)} %pad_maximum_fusion.6), channel_id=1, source_target_pairs={{0,2},{2,4},{4,6},{6,0},{1,3},{3,5},{5,7},{7,1},{8,10},{10,12},{12... | collective-permute-start | bytes 688136 | tf_op jit(solution)/shard_map/line_weights/ppermute | solution.py:28
  5.3 2.5 %collective-permute-start.1 = (bf16[56,2048]{1,0:T(8,128)(2,1)}, bf16[56,2048]{1,0:T(8,128)(2,1)}, u32[]{:S(2)}, u32[]{:S(2)}) collective-permute-start(bf16[56,2048]{1,0:T(8,128)(2,1)} %pad_maximum_fusion.6), channel_id=1, source_target_pairs={{0,4},{2,6},{4,0},{6,2},{1,5},{3,7},{5,1},{7,3},{8,12},{10,14},{12... | collective-permute-start | bytes 688136 | tf_op jit(solution)/shard_map/line_weights/ppermute | solution.py:28
  7.8 1.2 collective-permute-start
  13.6 11.2 %all-to-all-start = ((bf16[32,2,136]{2,1,0:T(2,128)(2,1)}), bf16[32,2,136]{2,1,0:T(2,128)(2,1)S(1)}, u32[]{:S(2)}, u32[]{:S(2)}) async-start(bf16[32,2,136]{2,1,0:T(2,128)(2,1)} %maximum_bitcast_fusion), calls=%async_computation | async-start | bytes 65536 | tf_op jit(solution)/shard_map/spread_tokens/all_to_all | solution.py:23
  24.8 0.9 fusion.102
  26.4 1.5 %fusion.19 = bf16[2,1,256]{2,0,1:T(2,128)(2,1)S(1)} fusion(bf16[2,2048]{1,0:T(2,128)(2,1)S(1)} %fusion.45, bf16[2048,256]{1,0:T(8,128)(2,1)} %param.34), kind=kOutput, calls=%fused_computation.25 | convolution fusion | flops 2097664 | bytes 1057792 | tf_op jit(solution)/shard_map/dot_general | solution.py:182
  28.9 4.6 %all-to-all-done = bf16[32,2,136]{2,1,0:T(2,128)(2,1)S(1)} async-done(((bf16[32,2,136]{2,1,0:T(2,128)(2,1)}), bf16[32,2,136]{2,1,0:T(2,128)(2,1)S(1)}, u32[]{:S(2)}, u32[]{:S(2)}) %all-to-all-start) | async-done | bytes 17440 | tf_op jit(solution)/shard_map/spread_tokens/all_to_all | solution.py:23
  33.5 1.8 %pad_maximum_fusion.4 = (bf16[4,16,2048]{2,1,0:T(8,128)(2,1)S(1)}, bf16[4,16,2048]{2,1,0:T(8,128)(2,1)S(1)}, bf16[4,16,2048]{2,1,0:T(8,128)(2,1)}) fusion(bf16[1,56,2048]{2,1,0:T(8,128)(2,1)} %bitcast.7, bf16[1,56,2048]{2,1,0:T(8,128)(2,1)} %bitcast.6, bf16[1,56,2048]{2,1,0:T(8,128)(2,1)} %bitcast.5, bf16[1,56,2048]{2,1,0:T(8,128)(2,1)S(1)} %fusion.102), kind=kLoop, calls=%fused_computation.45 | loop fusion | flops 3145728 | bytes 1703936 | tf_op jit(solution)/shard_map/slice | solution.py:173
  36.7 4.6 %all-to-all-start.1 = ((bf16[32,2,2048]{2,1,0:T(2,128)(2,1)}), bf16[32,2,2048]{2,1,0:T(2,128)(2,1)S(1)}, u32[]{:S(2)}, u32[]{:S(2)}) async-start(bf16[32,2,2048]{2,1,0:T(2,128)(2,1)} %reshape.263), calls=%async_computation.1 | async-start | bytes 524288 | tf_op jit(solution)/shard_map/in_proj/all_to_all | solution.py:23
  41.6 10.1 %all-to-all-done.1 = bf16[32,2,2048]{2,1,0:T(2,128)(2,1)S(1)} async-done(((bf16[32,2,2048]{2,1,0:T(2,128)(2,1)}), bf16[32,2,2048]{2,1,0:T(2,128)(2,1)S(1)}, u32[]{:S(2)}, u32[]{:S(2)}) %all-to-all-start.1) | async-done | bytes 262176 | tf_op jit(solution)/shard_map/in_proj/all_to_all | solution.py:23
  52.2 2.6 %multiply_reduce_fusion.1 = (f32[2,16,64]{2,1,0:T(8,128)S(1)}, f32[2,16,64,128]{3,2,1,0:T(8,128)}) fusion(f32[2,16,128]{2,1,0:T(8,128)S(1)} %get-tuple-element.28, f32[2,16,128]{2,1,0:T(8,128)S(1)} %get-tuple-element.29, f32[2,16,64]{2,1,0:T(8,128)S(1)} %multiply_multiply_fusion, f32[2,16,64,128]{3,2,1,0:T(8,128)} %param.27, f32[2,16]{1,0:T(2,128)S(1)} %get-tuple-element.26), kind=kLoop, calls=%fused_computation.31 | loop fusion | flops 1308672 | bytes 2146432 | tf_op jit(solution)/shard_map/state/reduce_sum | solution.py:85
  55.9 3.8 %all-to-all-start.2 = ((bf16[32,2,1024]{2,1,0:T(2,128)(2,1)}), bf16[32,2,1024]{2,1,0:T(2,128)(2,1)S(1)}, u32[]{:S(2)}, u32[]{:S(2)}) async-start(bf16[32,2,1024]{2,1,0:T(2,128)(2,1)} %broadcast_in_dim.47), calls=%async_computation.2 | async-start | bytes 262144 | tf_op jit(solution)/shard_map/out_proj/all_to_all | solution.py:23
  60.7 8.4 %all-to-all-done.2 = bf16[32,2,1024]{2,1,0:T(2,128)(2,1)S(1)} async-done(((bf16[32,2,1024]{2,1,0:T(2,128)(2,1)}), bf16[32,2,1024]{2,1,0:T(2,128)(2,1)S(1)}, u32[]{:S(2)}, u32[]{:S(2)}) %all-to-all-start.2) | async-done | bytes 131104 | tf_op jit(solution)/shard_map/out_proj/all_to_all | solution.py:23
  69.5 4.9 %collective-permute-start.3 = (f32[64,64]{1,0:T(8,128)S(1)}, f32[64,64]{1,0:T(8,128)S(1)}, u32[]{:S(2)}, u32[]{:S(2)}) collective-permute-start(f32[64,64]{1,0:T(8,128)S(1)} %fusion.17), channel_id=1, source_target_pairs={{0,1},{1,0},{2,3},{3,2},{4,5},{5,4},{6,7},{7,6},{8,9},{9,8},{10,11... | collective-permute-start | bytes 49160 | tf_op jit(solution)/shard_map/out_proj/ppermute | solution.py:28
  75.4 1.1 reshape.270
  76.6 3.9 %all-to-all-start.3 = ((bf16[32,2,2048]{2,1,0:T(2,128)(2,1)}), bf16[32,2,2048]{2,1,0:T(2,128)(2,1)S(1)}, u32[]{:S(2)}, u32[]{:S(2)}) async-start(bf16[32,2,2048]{2,1,0:T(2,128)(2,1)} %reshape.270), calls=%async_computation.3 | async-start | bytes 524288 | tf_op jit(solution)/shard_map/hidden/all_to_all | solution.py:23
  81.4 10.9 %all-to-all-done.3 = bf16[32,2,2048]{2,1,0:T(2,128)(2,1)S(1)} async-done(((bf16[32,2,2048]{2,1,0:T(2,128)(2,1)}), bf16[32,2,2048]{2,1,0:T(2,128)(2,1)S(1)}, u32[]{:S(2)}, u32[]{:S(2)}) %all-to-all-start.3) | async-done | bytes 262176 | tf_op jit(solution)/shard_map/hidden/all_to_all | solution.py:23
  94.2 2.0 %collective-permute-start.5 = (bf16[32,2048]{1,0:T(8,128)(2,1)S(1)}, bf16[32,2048]{1,0:T(8,128)(2,1)S(1)}, u32[]{:S(2)}, u32[]{:S(2)}) collective-permute-start(bf16[32,2048]{1,0:T(8,128)(2,1)S(1)} %get-tuple-element.19), channel_id=1, source_target_pairs={{0,4},{2,6},{4,0},{6,2},{1,5},{3,7},{5,1},{7,3},{8,12},{10,14},{12... | collective-permute-start | bytes 393224 | tf_op jit(solution)/shard_map/dispatch/ppermute | solution.py:28
  96.2 1.7 %collective-permute-done.6 = bf16[32,2048]{1,0:T(8,128)(2,1)S(1)} collective-permute-done((bf16[32,2048]{1,0:T(8,128)(2,1)S(1)}, bf16[32,2048]{1,0:T(8,128)(2,1)S(1)}, u32[]{:S(2)}, u32[]{:S(2)}) %collective-permute-start.6) | collective-permute-done | bytes 131104 | tf_op jit(solution)/shard_map/dispatch/ppermute | solution.py:28
  97.9 1.6 %collective-permute-done.5 = bf16[32,2048]{1,0:T(8,128)(2,1)S(1)} collective-permute-done((bf16[32,2048]{1,0:T(8,128)(2,1)S(1)}, bf16[32,2048]{1,0:T(8,128)(2,1)S(1)}, u32[]{:S(2)}, u32[]{:S(2)}) %collective-permute-start.5) | collective-permute-done | bytes 131104 | tf_op jit(solution)/shard_map/dispatch/ppermute | solution.py:28
  99.5 2.3 %collective-permute-done.4 = bf16[32,2048]{1,0:T(8,128)(2,1)S(1)} collective-permute-done((bf16[32,2048]{1,0:T(8,128)(2,1)S(1)}, bf16[32,2048]{1,0:T(8,128)(2,1)S(1)}, u32[]{:S(2)}, u32[]{:S(2)}) %collective-permute-start.4) | collective-permute-done | bytes 131104 | tf_op jit(solution)/shard_map/dispatch/ppermute | solution.py:28
  102.5 1.2 fusion.8
  103.7 3.4 %convolution_convert_fusion = bf16[128,2048]{1,0:T(8,128)(2,1)} fusion(bf16[1,512,2048]{2,1,0:T(8,128)(2,1)S(1)} %copy-done, f32[128,512]{1,0:T(8,128)} %fusion.8, bf16[1,2048,512]{2,1,0:T(8,128)(2,1)} %param.47, bf16[32,2048]{1,0:T(8,128)(2,1)} %copy-done.11, bf16[32,2048]{1,0:T(8,128)(2,1)} %copy-done.12, bf16[32,2048]{1,0:T(8,128)(2,1)} %copy-done.13, ...), kind=kOutput, calls=%fused_computation | convolution fusion | flops 539820032 | bytes 5505024 | tf_op jit(solution)/shard_map/expert/dot_general | solution.py:248
  107.0 1.8 %fusion.79 = (bf16[32,2048]{1,0:T(8,128)(2,1)S(1)}, bf16[32,2048]{1,0:T(8,128)(2,1)}, bf16[32,2048]{1,0:T(8,128)(2,1)}, bf16[32,2048]{1,0:T(8,128)(2,1)}) fusion(bf16[128,2048]{1,0:T(8,128)(2,1)} %convolution_convert_fusion), kind=kLoop, calls=%fused_computation.133 | loop fusion | bytes 1048576 | tf_op jit(solution)/shard_map/expert/slice | solution.py:251
  108.9 2.0 %collective-permute-start.8 = (bf16[32,2048]{1,0:T(8,128)(2,1)}, bf16[32,2048]{1,0:T(8,128)(2,1)}, u32[]{:S(2)}, u32[]{:S(2)}) collective-permute-start(bf16[32,2048]{1,0:T(8,128)(2,1)} %get-tuple-element.15), channel_id=1, source_target_pairs={{0,4},{2,6},{4,0},{6,2},{1,5},{3,7},{5,1},{7,3},{8,12},{10,14},{12... | collective-permute-start | bytes 393224 | tf_op jit(solution)/shard_map/expert/ppermute | solution.py:28
  111.6 2.2 %convolution_multiply_fusion = f32[64,2048]{1,0:T(8,128)} fusion(bf16[64,2048]{1,0:T(8,128)(2,1)} %bitcast.95, f32[64]{0:T(128)S(1)} %add_divide_fusion, bf16[64,2048]{1,0:T(8,128)(2,1)S(1)} %bitcast.94, bf16[2048,64]{1,0:T(8,128)(2,1)S(1)} %bitcast.92), kind=kOutput, calls=%fused_computation.3 | convolution fusion | flops 33705984 | bytes 1310976 | tf_op jit(solution)/shard_map/dense/dot_general | solution.py:263
  113.8 1.8 %collective-permute-done.9 = bf16[32,2048]{1,0:T(8,128)(2,1)} collective-permute-done((bf16[32,2048]{1,0:T(8,128)(2,1)}, bf16[32,2048]{1,0:T(8,128)(2,1)}, u32[]{:S(2)}, u32[]{:S(2)}) %collective-permute-start.9) | collective-permute-done | bytes 131104 | tf_op jit(solution)/shard_map/expert/ppermute | solution.py:28
  116.3 1.5 %fusion.1 = bf16[64,1,2048]{2,0,1:T(8,128)(2,1)S(1)} fusion(f32[64,2048]{1,0:T(8,128)} %convolution_multiply_fusion, bf16[128,64]{1,0:T(8,128)(2,1)} %fusion.38, bf16[32,2048]{1,0:T(8,128)(2,1)} %collective-permute-done.9, bf16[32,2048]{1,0:T(8,128)(2,1)} %collective-permute-done.8, bf16[32,2048]{1,0:T(8,128)(2,1)} %collective-permute-done.7, ...), kind=kOutput, calls=%fused_computation.7 | convolution fusion | flops 35913728 | bytes 1327104 | tf_op jit(solution)/shard_map/combine/dot_general | solution.py:269
  119.9 9.7 %all-to-all-start.4 = ((bf16[64,2,1024]{2,1,0:T(2,128)(2,1)}), bf16[64,2,1024]{2,1,0:T(2,128)(2,1)S(1)}, u32[]{:S(2)}, u32[]{:S(2)}) async-start(bf16[64,2,1024]{2,1,0:T(2,128)(2,1)} %reshape.272), calls=%async_computation.4 | async-start | bytes 524288 | tf_op jit(solution)/shard_map/combine/all_to_all | solution.py:23
  130.8 11.9 %all-to-all-done.4 = bf16[64,2,1024]{2,1,0:T(2,128)(2,1)S(1)} async-done(((bf16[64,2,1024]{2,1,0:T(2,128)(2,1)}), bf16[64,2,1024]{2,1,0:T(2,128)(2,1)S(1)}, u32[]{:S(2)}, u32[]{:S(2)}) %all-to-all-start.4) | async-done | bytes 262176 | tf_op jit(solution)/shard_map/combine/all_to_all | solution.py:23
  (124 shorter events, 21.4 us)
Async XLA Ops:
  0.6 103.0 %copy-start = (bf16[1,512,2048]{2,1,0:T(8,128)(2,1)S(1)}, bf16[1,512,2048]{2,1,0:T(8,128)(2,1)}, u32[]{:S(2)}) copy-start(bf16[1,512,2048]{2,1,0:T(8,128)(2,1)} %param.48) | copy-start | bytes 6291460
  0.6 27.2 %copy-start.1 = (bf16[2048,256]{1,0:T(8,128)(2,1)S(1)}, bf16[2048,256]{1,0:T(8,128)(2,1)}, u32[]{:S(2)}) copy-start(bf16[2048,256]{1,0:T(8,128)(2,1)} %param.33) | copy-start | bytes 3145732
  0.7 27.5 %copy-start.7 = (f32[4,2,256]{2,1,0:T(2,128)S(1)}, f32[4,2,256]{2,1,0:T(2,128)}, u32[]{:S(2)}) copy-start(f32[4,2,256]{2,1,0:T(2,128)} %param.37) | copy-start | bytes 24580
  0.7 27.6 %copy-start.15 = (f32[16]{0:T(128)S(1)}, f32[16]{0:T(128)}, u32[]{:S(2)}) copy-start(f32[16]{0:T(128)} %param.39) | copy-start | bytes 196
  0.7 27.6 %copy-start.16 = (f32[16]{0:T(128)S(1)}, f32[16]{0:T(128)}, u32[]{:S(2)}) copy-start(f32[16]{0:T(128)} %param.38) | copy-start | bytes 196
  0.7 27.8 %copy-start.5 = (f32[2048]{0:T(1024)S(1)}, f32[2048]{0:T(1024)}, u32[]{:S(2)}) copy-start(f32[2048]{0:T(1024)} %param.51) | copy-start | bytes 24580
  0.7 27.9 %copy-start.6 = (f32[2048]{0:T(1024)S(1)}, f32[2048]{0:T(1024)}, u32[]{:S(2)}) copy-start(f32[2048]{0:T(1024)} %param.43) | copy-start | bytes 24580
  0.7 27.9 %copy-start.9 = (f32[16]{0:T(128)S(1)}, f32[16]{0:T(128)}, u32[]{:S(2)}) copy-start(f32[16]{0:T(128)} %param.40) | copy-start | bytes 196
  3.3 30.2 %collective-permute-start.2 = (bf16[56,2048]{1,0:T(8,128)(2,1)}, bf16[56,2048]{1,0:T(8,128)(2,1)}, u32[]{:S(2)}, u32[]{:S(2)}) collective-permute-start(bf16[56,2048]{1,0:T(8,128)(2,1)} %pad_maximum_fusion.6), channel_id=1, source_target_pairs={{0,2},{2,4},{4,6},{6,0},{1,3},{3,5},{5,7},{7,1},{8,10},{10,12},{12... | collective-permute-start | bytes 688136 | tf_op jit(solution)/shard_map/line_weights/ppermute | solution.py:28
  5.3 28.2 %collective-permute-start.1 = (bf16[56,2048]{1,0:T(8,128)(2,1)}, bf16[56,2048]{1,0:T(8,128)(2,1)}, u32[]{:S(2)}, u32[]{:S(2)}) collective-permute-start(bf16[56,2048]{1,0:T(8,128)(2,1)} %pad_maximum_fusion.6), channel_id=1, source_target_pairs={{0,4},{2,6},{4,0},{6,2},{1,5},{3,7},{5,1},{7,3},{8,12},{10,14},{12... | collective-permute-start | bytes 688136 | tf_op jit(solution)/shard_map/line_weights/ppermute | solution.py:28
  7.8 25.8 %collective-permute-start = (bf16[56,2048]{1,0:T(8,128)(2,1)}, bf16[56,2048]{1,0:T(8,128)(2,1)}, u32[]{:S(2)}, u32[]{:S(2)}) collective-permute-start(bf16[56,2048]{1,0:T(8,128)(2,1)} %pad_maximum_fusion.6), channel_id=1, source_target_pairs={{0,6},{2,0},{4,2},{6,4},{1,7},{3,1},{5,3},{7,5},{8,14},{10,8},{12,... | collective-permute-start | bytes 688136 | tf_op jit(solution)/shard_map/line_weights/ppermute | solution.py:28
  13.6 19.9 %all-to-all-start = ((bf16[32,2,136]{2,1,0:T(2,128)(2,1)}), bf16[32,2,136]{2,1,0:T(2,128)(2,1)S(1)}, u32[]{:S(2)}, u32[]{:S(2)}) async-start(bf16[32,2,136]{2,1,0:T(2,128)(2,1)} %maximum_bitcast_fusion), calls=%async_computation | async-start | bytes 65536 | tf_op jit(solution)/shard_map/spread_tokens/all_to_all | solution.py:23
  24.8 3.5 %copy-start.14 = (bf16[2048,16]{0,1:T(8,128)(2,1)S(1)}, bf16[2048,16]{0,1:T(8,128)(2,1)}, u32[]{:S(2)}) copy-start(bf16[2048,16]{0,1:T(8,128)(2,1)} %param.35) | copy-start | bytes 196612
  28.1 23.8 %copy-start.2 = (bf16[2,3,1024]{2,0,1:T(2,128)(2,1)S(1)}, bf16[2,3,1024]{2,0,1:T(2,128)(2,1)}, u32[]{:S(2)}) copy-start(bf16[2,3,1024]{2,0,1:T(2,128)(2,1)} %param.28) | copy-start | bytes 36868
  28.1 23.8 %copy-start.4 = (f32[4,1024]{1,0:T(4,128)S(1)}, f32[4,1024]{1,0:T(4,128)}, u32[]{:S(2)}) copy-start(f32[4,1024]{1,0:T(4,128)} %param.36) | copy-start | bytes 49156
  35.4 19.7 %copy-start.8 = (f32[1024]{0:T(1024)S(1)}, f32[1024]{0:T(1024)}, u32[]{:S(2)}) copy-start(f32[1024]{0:T(1024)} %param.41) | copy-start | bytes 12292
  36.7 15.0 %all-to-all-start.1 = ((bf16[32,2,2048]{2,1,0:T(2,128)(2,1)}), bf16[32,2,2048]{2,1,0:T(2,128)(2,1)S(1)}, u32[]{:S(2)}, u32[]{:S(2)}) async-start(bf16[32,2,2048]{2,1,0:T(2,128)(2,1)} %reshape.263), calls=%async_computation.1 | async-start | bytes 524288 | tf_op jit(solution)/shard_map/in_proj/all_to_all | solution.py:23
  55.9 13.2 %all-to-all-start.2 = ((bf16[32,2,1024]{2,1,0:T(2,128)(2,1)}), bf16[32,2,1024]{2,1,0:T(2,128)(2,1)S(1)}, u32[]{:S(2)}, u32[]{:S(2)}) async-start(bf16[32,2,1024]{2,1,0:T(2,128)(2,1)} %broadcast_in_dim.47), calls=%async_computation.2 | async-start | bytes 262144 | tf_op jit(solution)/shard_map/out_proj/all_to_all | solution.py:23
  69.5 5.8 %collective-permute-start.3 = (f32[64,64]{1,0:T(8,128)S(1)}, f32[64,64]{1,0:T(8,128)S(1)}, u32[]{:S(2)}, u32[]{:S(2)}) collective-permute-start(f32[64,64]{1,0:T(8,128)S(1)} %fusion.17), channel_id=1, source_target_pairs={{0,1},{1,0},{2,3},{3,2},{4,5},{5,4},{6,7},{7,6},{8,9},{9,8},{10,11... | collective-permute-start | bytes 49160 | tf_op jit(solution)/shard_map/out_proj/ppermute | solution.py:28
  76.6 15.7 %all-to-all-start.3 = ((bf16[32,2,2048]{2,1,0:T(2,128)(2,1)}), bf16[32,2,2048]{2,1,0:T(2,128)(2,1)S(1)}, u32[]{:S(2)}, u32[]{:S(2)}) async-start(bf16[32,2,2048]{2,1,0:T(2,128)(2,1)} %reshape.270), calls=%async_computation.3 | async-start | bytes 524288 | tf_op jit(solution)/shard_map/hidden/all_to_all | solution.py:23
  92.6 9.9 %copy-start.10 = (bf16[1,2048,512]{2,1,0:T(8,128)(2,1)S(1)}, bf16[1,2048,512]{2,1,0:T(8,128)(2,1)}, u32[]{:S(2)}) copy-start(bf16[1,2048,512]{2,1,0:T(8,128)(2,1)} %param.46) | copy-start | bytes 6291460
  94.0 3.9 %collective-permute-start.6 = (bf16[32,2048]{1,0:T(8,128)(2,1)S(1)}, bf16[32,2048]{1,0:T(8,128)(2,1)S(1)}, u32[]{:S(2)}, u32[]{:S(2)}) collective-permute-start(bf16[32,2048]{1,0:T(8,128)(2,1)S(1)} %get-tuple-element.18), channel_id=1, source_target_pairs={{0,6},{2,0},{4,2},{6,4},{1,7},{3,1},{5,3},{7,5},{8,14},{10,8},{12,... | collective-permute-start | bytes 393224 | tf_op jit(solution)/shard_map/dispatch/ppermute | solution.py:28
  94.2 5.3 %collective-permute-start.5 = (bf16[32,2048]{1,0:T(8,128)(2,1)S(1)}, bf16[32,2048]{1,0:T(8,128)(2,1)S(1)}, u32[]{:S(2)}, u32[]{:S(2)}) collective-permute-start(bf16[32,2048]{1,0:T(8,128)(2,1)S(1)} %get-tuple-element.19), channel_id=1, source_target_pairs={{0,4},{2,6},{4,0},{6,2},{1,5},{3,7},{5,1},{7,3},{8,12},{10,14},{12... | collective-permute-start | bytes 393224 | tf_op jit(solution)/shard_map/dispatch/ppermute | solution.py:28
  96.2 5.6 %collective-permute-start.4 = (bf16[32,2048]{1,0:T(8,128)(2,1)S(1)}, bf16[32,2048]{1,0:T(8,128)(2,1)S(1)}, u32[]{:S(2)}, u32[]{:S(2)}) collective-permute-start(bf16[32,2048]{1,0:T(8,128)(2,1)S(1)} %get-tuple-element.20), channel_id=1, source_target_pairs={{0,2},{2,4},{4,6},{6,0},{1,3},{3,5},{5,7},{7,1},{8,10},{10,12},{12... | collective-permute-start | bytes 393224 | tf_op jit(solution)/shard_map/dispatch/ppermute | solution.py:28
  97.9 3.9 %copy-start.11 = (bf16[32,2048]{1,0:T(8,128)(2,1)}, bf16[32,2048]{1,0:T(8,128)(2,1)S(1)}, u32[]{:S(2)}) copy-start(bf16[32,2048]{1,0:T(8,128)(2,1)S(1)} %collective-permute-done.6) | copy-start | bytes 393220
  99.5 2.3 %copy-start.12 = (bf16[32,2048]{1,0:T(8,128)(2,1)}, bf16[32,2048]{1,0:T(8,128)(2,1)S(1)}, u32[]{:S(2)}) copy-start(bf16[32,2048]{1,0:T(8,128)(2,1)S(1)} %collective-permute-done.5) | copy-start | bytes 393220
  101.8 0.7 copy-start.13
  108.9 6.7 %collective-permute-start.9 = (bf16[32,2048]{1,0:T(8,128)(2,1)}, bf16[32,2048]{1,0:T(8,128)(2,1)}, u32[]{:S(2)}, u32[]{:S(2)}) collective-permute-start(bf16[32,2048]{1,0:T(8,128)(2,1)} %get-tuple-element.14), channel_id=1, source_target_pairs={{0,2},{2,4},{4,6},{6,0},{1,3},{3,5},{5,7},{7,1},{8,10},{10,12},{12... | collective-permute-start | bytes 393224 | tf_op jit(solution)/shard_map/expert/ppermute | solution.py:28
  108.9 6.7 %collective-permute-start.8 = (bf16[32,2048]{1,0:T(8,128)(2,1)}, bf16[32,2048]{1,0:T(8,128)(2,1)}, u32[]{:S(2)}, u32[]{:S(2)}) collective-permute-start(bf16[32,2048]{1,0:T(8,128)(2,1)} %get-tuple-element.15), channel_id=1, source_target_pairs={{0,4},{2,6},{4,0},{6,2},{1,5},{3,7},{5,1},{7,3},{8,12},{10,14},{12... | collective-permute-start | bytes 393224 | tf_op jit(solution)/shard_map/expert/ppermute | solution.py:28
  110.9 5.4 %collective-permute-start.7 = (bf16[32,2048]{1,0:T(8,128)(2,1)}, bf16[32,2048]{1,0:T(8,128)(2,1)}, u32[]{:S(2)}, u32[]{:S(2)}) collective-permute-start(bf16[32,2048]{1,0:T(8,128)(2,1)} %get-tuple-element.16), channel_id=1, source_target_pairs={{0,6},{2,0},{4,2},{6,4},{1,7},{3,1},{5,3},{7,5},{8,14},{10,8},{12,... | collective-permute-start | bytes 393224 | tf_op jit(solution)/shard_map/expert/ppermute | solution.py:28
  113.8 16.4 %copy-start.3 = (bf16[2,3,1024]{2,0,1:T(2,128)(2,1)S(1)}, bf16[2,3,1024]{2,0,1:T(2,128)(2,1)}, u32[]{:S(2)}) copy-start(bf16[2,3,1024]{2,0,1:T(2,128)(2,1)} %param.28) | copy-start | bytes 36868
  119.9 22.7 %all-to-all-start.4 = ((bf16[64,2,1024]{2,1,0:T(2,128)(2,1)}), bf16[64,2,1024]{2,1,0:T(2,128)(2,1)S(1)}, u32[]{:S(2)}, u32[]{:S(2)}) async-start(bf16[64,2,1024]{2,1,0:T(2,128)(2,1)} %reshape.272), calls=%async_computation.4 | async-start | bytes 524288 | tf_op jit(solution)/shard_map/combine/all_to_all | solution.py:23

commit v2 on v1

v2 whole, which is shorter than its diff:
```python
import jax
import jax.numpy as jnp
from jax import lax
from jax.experimental import pallas as pl
from jax.experimental.pallas import tpu as pltpu
from jax.sharding import Mesh
from jax.sharding import PartitionSpec as P

GROUPS = 4
ROW_AXES = ("z", "y")
EP = ("z", "y", "x")
EP_TP = ("z", "y", "x", "tp")


norm_eps = 1e-05
clamp_limit = 7.0
glu_alpha = 1.702
f32 = jnp.float32
bf16 = jnp.bfloat16


def in_vmem(*arrays):
    return [pltpu.with_memory_space_constraint(a, pltpu.VMEM) for a in arrays]


def in_hbm(*arrays):
    return [pltpu.with_memory_space_constraint(a, pltpu.HBM) for a in arrays]


def exchanged(pieces, axis):
    return lax.all_to_all(pieces, axis, split_axis=0, concat_axis=0, tiled=True)


def shifted(block, axis, by):
    size = lax.axis_size(axis)
    return lax.ppermute(block, axis, [(i, (i + by) % size) for i in range(size)])


def rms_scale(values, gain_vec):
    return (
        values * lax.rsqrt(jnp.mean(values * values, axis=-1, keepdims=True) + norm_eps) * gain_vec
    )


def clamped_unit(gate_pre, up_pre):
    glu_part = jnp.minimum(gate_pre, clamp_limit)
    lin_part = jnp.clip(up_pre, -clamp_limit, clamp_limit)
    return glu_part * jax.nn.sigmoid(glu_alpha * glu_part) * (lin_part + 1.0)


def start_kernel(
    tokens,
    gain,
    routes,
    logits,
    gate_weight,
    inner_weight,
    down,
    up,
    out,
    features,
    normed_out,
    held,
    extra,
):
    seq_count, width = tokens.shape
    share, channels = gate_weight.shape
    topk = routes.shape[1]
    half = share // 2
    held[:share, :channels] = gate_weight[...]
    held[:share, channels:] = inner_weight[...]
    held[share : 2 * share, :] = down[...]
    held[2 * share : 3 * share, :] = up[...]
    held[3 * share :, :channels] = out[:half, :]
    held[3 * share :, channels:] = out[half:, :]
    raw = tokens[...].astype(f32)
    normed = rms_scale(raw, gain[...]).astype(bf16)
    normed_out[...] = normed
    normed = normed.astype(f32)
    extra[...] = jnp.zeros(extra.shape, f32)
    extra[:, :topk] = routes[...].astype(f32)
    extra[:, topk : 2 * topk] = logits[...].astype(f32)
    tail = extra[...].astype(bf16)
    first = lax.broadcasted_iota(jnp.int32, (seq_count, 128), 1) < 64
    for pair in range(width // 128):
        at = slice(128 * pair, 128 * pair + 128)
        features[2 * pair, :, :128] = jnp.where(
            first, normed[:, at], pltpu.roll(raw[:, at], 64, 1)
        ).astype(bf16)
        features[2 * pair + 1, :, :128] = jnp.where(
            first, pltpu.roll(normed[:, at], 64, 1), raw[:, at]
        ).astype(bf16)
        features[2 * pair, :, 128:] = tail
        features[2 * pair + 1, :, 128:] = tail


def in_kernel(line_at, spread, h0, h1, h2, h3, part):
    share = h0.shape[0] // 7 * 2
    block = 4 * share
    row = lax.broadcasted_iota(jnp.int32, (block, block), 0)
    column = lax.broadcasted_iota(jnp.int32, (block, block), 1)
    turn = (row == (column + share * line_at[0]) % block).astype(bf16)
    turned = jnp.dot(spread[:, :block], turn, preferred_element_type=f32).astype(bf16)
    weight = jnp.concatenate([h[:share, :] for h in (h0, h1, h2, h3)], axis=0)
    part[...] = jnp.dot(turned, weight, preferred_element_type=f32).astype(bf16)


def dispatch_kernel(picks, hidden, gain, r0, r1, r2, r3):
    rows = lax.dot_general(
        picks[...], hidden[...], (((1,), (1,)), ((), ())), preferred_element_type=f32
    )
    rows = rms_scale(rows, gain[...]).astype(bf16)
    count = r0.shape[0]
    for n, ref in enumerate((r0, r1, r2, r3)):
        ref[...] = rows[n * count : (n + 1) * count]


def dense_kernel(
    own_at,
    hidden,
    gain,
    dense_gate,
    h0,
    h1,
    h2,
    h3,
    expert_gate,
    expert_up,
    term,
    own,
    gate_near,
    up_near,
    sems,
):
    copies = (
        pltpu.make_async_copy(expert_gate.at[0], gate_near, sems.at[0]),
        pltpu.make_async_copy(expert_up.at[0], up_near, sems.at[1]),
    )
    for copy in copies:
        copy.start()
    share = h0.shape[0] // 7 * 2
    batch = hidden.shape[1]
    row = lax.broadcasted_iota(jnp.int32, (batch, batch), 0)
    column = lax.broadcasted_iota(jnp.int32, (batch, batch), 1)
    rows = lax.dot_general(
        (row == column).astype(bf16),
        hidden[...],
        (((1,), (1,)), ((), ())),
        preferred_element_type=f32,
    )
    at = lax.broadcasted_iota(jnp.int32, rows.shape, 0)
    own[...] = jnp.sum(jnp.where(at == own_at[0], rows, 0.0), axis=0, keepdims=True)
    normed = rms_scale(rows, gain[...]).astype(bf16)
    weight = jax.nn.sigmoid(
        jnp.sum(normed.astype(f32) * dense_gate[...], axis=-1, keepdims=True)
    )
    helds = (h0, h1, h2, h3)
    down = jnp.concatenate([h[share : 2 * share, :] for h in helds], axis=0)
    up = jnp.concatenate([h[2 * share : 3 * share, :] for h in helds], axis=0)
    inner = jax.nn.silu(
        lax.dot_general(normed, up, (((1,), (1,)), ((), ())), preferred_element_type=f32)
    ).astype(bf16)
    term[...] = jnp.dot(inner, down, preferred_element_type=f32) * weight
    for copy in copies:
        copy.wait()


def combine_kernel(placed, dense_term, e0, e1, e2, e3, terms):
    rows = jnp.concatenate([e0[...], e1[...], e2[...], e3[...]], axis=0)
    mix = jnp.dot(placed[...], rows, preferred_element_type=f32)
    terms[...] = (mix + dense_term[...]).astype(bf16)


def expert_kernel(own, one, two, three, gate, up, down, r0, r1, r2, r3, down_near, sems):
    _, width = down_near.shape
    parts = sems.shape[0]
    piece = width // parts
    copies = []
    for k in range(parts):
        at = pl.ds(k * piece, piece)
        copies.append(pltpu.make_async_copy(down.at[0, :, at], down_near.at[:, at], sems.at[k]))
    for copy in copies:
        copy.start()
    rows = jnp.concatenate([own[...], one[...], two[...], three[...]], axis=0)
    activated = clamped_unit(
        jnp.dot(rows, gate[...], preferred_element_type=f32),
        jnp.dot(rows, up[...], preferred_element_type=f32),
    ).astype(bf16)
    count = own.shape[0]
    for k in range(parts):
        copies[k].wait()
        at = slice(k * piece, (k + 1) * piece)
        result = jnp.dot(activated, down_near[:, at], preferred_element_type=f32).astype(bf16)
        for n, ref in enumerate((r0, r1, r2, r3)):
            ref[:, at] = result[n * count : (n + 1) * count]


def state_step(
    inner_proj,
    gate_proj,
    write_proj,
    read_proj,
    step_raw,
    conv_state,
    conv_proj_state,
    conv_kernel,
    conv_proj_kernel,
    step_bias,
    log_rate,
    skip_gain,
    group_gain,
    head_state,
    group_count,
):
    window_inner = jnp.concatenate([conv_state, inner_proj[:, None, :]], axis=1)
    window_proj = jnp.concatenate(
        [conv_proj_state, jnp.stack([write_proj, read_proj], axis=1)[:, None]], axis=1
    )
    conv_inner = jax.nn.silu(jnp.sum(window_inner.astype(f32) * conv_kernel[None], axis=1))
    conv_proj = jax.nn.silu(jnp.sum(window_proj.astype(f32) * conv_proj_kernel[None], axis=1))
    seq_count, channels = conv_inner.shape
    head_count = step_raw.shape[1]
    head_width = channels // head_count
    state_width = conv_proj.shape[2] // group_count
    per_group = head_count // group_count
    head_input = conv_inner.reshape(seq_count, head_count, head_width)
    write_heads = jnp.repeat(
        conv_proj[:, 0].reshape(seq_count, group_count, state_width), per_group, axis=1
    )
    read_heads = jnp.repeat(
        conv_proj[:, 1].reshape(seq_count, group_count, state_width), per_group, axis=1
    )
    step_size = jax.nn.softplus(step_raw + step_bias)
    decay_rate = jnp.exp(-jnp.exp(log_rate) * step_size)
    state_out = (
        decay_rate[:, :, None, None] * head_state
        + (step_size[:, :, None] * head_input)[:, :, :, None] * write_heads[:, :, None, :]
    )
    read_out = (
        jnp.sum(state_out * read_heads[:, :, None, :], axis=-1)
        + skip_gain[None, :, None] * head_input
    )
    gated_rows = read_out.reshape(seq_count, channels) * jax.nn.silu(gate_proj.astype(f32))
    grouped = gated_rows.reshape(seq_count, group_count, channels // group_count)
    grouped = grouped * lax.rsqrt(jnp.mean(grouped * grouped, axis=-1, keepdims=True) + norm_eps)
    mixer_rows = (grouped.reshape(seq_count, channels) * group_gain).astype(bf16)
    return (mixer_rows, state_out, window_inner[:, 1:], window_proj[:, 1:])


def local(
    tokens,
    head_state,
    conv_state,
    conv_proj_state,
    first_gain,
    gate_weight,
    inner_weight,
    write_weight,
    read_weight,
    step_weight,
    conv_kernel,
    conv_proj_kernel,
    step_bias,
    log_rate,
    skip_gain,
    group_gain,
    out_weight,
    second_gain,
    routes,
    route_logits,
    expert_gate,
    expert_up,
    expert_down,
    dense_up,
    dense_down,
    dense_gate,
):
    seq_count, width = tokens.shape
    topk = routes.shape[1]
    capacity = 4 * seq_count * topk
    rows_n = lax.axis_size(ROW_AXES)
    line_n = lax.axis_size("x")
    row_at = lax.axis_index(ROW_AXES)
    line_at = lax.axis_index("x")
    tp_at = lax.axis_index("tp")
    share = gate_weight.shape[0]
    block = share * line_n
    batch = rows_n * seq_count
    channels = gate_weight.shape[1]

    smem = pl.BlockSpec(memory_space=pltpu.SMEM)
    vmem = pl.BlockSpec(memory_space=pltpu.VMEM)

    lanes = 2 * block + 128
    features, normed_in, held = pl.pallas_call(
        start_kernel,
        out_shape=(
            jax.ShapeDtypeStruct((rows_n, seq_count, lanes), bf16),
            jax.ShapeDtypeStruct((seq_count, width), bf16),
            jax.ShapeDtypeStruct((3 * share + share // 2, width), bf16),
        ),
        scratch_shapes=[pltpu.VMEM((seq_count, 128), f32)],
        name="start",
            compiler_params=pltpu.CompilerParams(vmem_limit_bytes=8 << 20),
    )(
        *in_hbm(
            tokens,
            first_gain[None],
            routes,
            route_logits,
            gate_weight,
            inner_weight,
            dense_down,
            dense_up.T,
            out_weight.T,
        )
    )
    spread = exchanged(features, ROW_AXES)
    spread = spread.reshape(batch, lanes)
    raw_block = spread[:, block : 2 * block]
    all_routes = spread[:, 2 * block : 2 * block + topk]
    all_logits = spread[:, 2 * block + topk : 2 * block + 2 * topk].astype(f32)

    lines = [held] + [shifted(held, "x", -by) for by in range(1, line_n)]
    order = jnp.arange(block, dtype=jnp.int32)
    unturn = ((order[:, None] - share * line_at) % block == order[None, :]).astype(bf16)

    def natural(part):
        return jnp.dot(unturn, part, preferred_element_type=f32).astype(bf16)

    line_out = natural(
        jnp.concatenate(
            [
                part[3 * share :, at : at + channels]
                for part in lines
                for at in (0, channels)
            ],
            axis=0,
        )
    )

    in_part = pl.pallas_call(
        in_kernel,
        out_shape=pltpu.VMEM((batch, width), bf16),
        in_specs=[smem] + [vmem] * (1 + line_n),
        out_specs=vmem,
        name="in_part",
        compiler_params=pltpu.CompilerParams(vmem_limit_bytes=8 << 20),
    )(line_at.reshape(1), *in_vmem(spread, *lines))
    in_terms = exchanged(in_part.reshape(rows_n, seq_count, 2 * channels), ROW_AXES)
    in_sum = jnp.sum(in_terms.astype(f32), axis=0).astype(bf16)
    gate_proj, inner_proj = in_sum[:, :channels], in_sum[:, channels:]
    write_proj = jnp.dot(normed_in, write_weight, preferred_element_type=f32).astype(bf16)
    read_proj = jnp.dot(normed_in, read_weight, preferred_element_type=f32).astype(bf16)
    step_raw = jnp.dot(normed_in, step_weight, preferred_element_type=f32)
    mixer_rows, state_out, conv_out, conv_proj_out = state_step(
        inner_proj,
        gate_proj,
        write_proj,
        read_proj,
        step_raw,
        conv_state,
        conv_proj_state,
        conv_kernel,
        conv_proj_kernel,
        step_bias,
        log_rate,
        skip_gain,
        group_gain,
        head_state,
        GROUPS // lax.axis_size("tp"),
    )
    mixer_all = exchanged(
        jnp.broadcast_to(mixer_rows, (rows_n, seq_count, channels)), ROW_AXES
    ).reshape(batch, channels)
    mixed_part = lax.dot_general(
        line_out, mixer_all, (((1,), (1,)), ((), ())), preferred_element_type=f32
    )
    mixed = mixed_part + shifted(mixed_part, "tp", 1)
    hidden_block = (raw_block.T.astype(f32) + mixed).astype(bf16)
    hidden = exchanged(
        jnp.broadcast_to(hidden_block, (rows_n, block, batch)), ROW_AXES
    ).reshape(width, batch)

    route_gates = jax.nn.softmax(all_logits, axis=-1)
    experts = (line_n * row_at + (line_at + jnp.arange(line_n)) % line_n).astype(bf16)
    hits = all_routes[None] == experts[:, None, None]
    row_weight = jnp.sum(jnp.where(hits, route_gates[None], 0.0), axis=2)
    chosen = jnp.any(hits, axis=2)
    earlier = (jnp.arange(batch)[:, None] < jnp.arange(batch)[None, :]).astype(bf16)
    slot = jnp.dot(chosen.astype(bf16), earlier, preferred_element_type=f32)
    slot_ids = jnp.arange(capacity, dtype=f32)
    picks = (slot[:, None, :] == slot_ids[None, :, None]) & chosen[:, None, :]
    placed = jnp.where(picks, row_weight[:, None, :], 0.0).astype(bf16)
    picks = picks.astype(bf16).reshape(line_n * capacity, batch)
    placed = placed.reshape(line_n * capacity, batch).T

    sent = pl.pallas_call(
        dispatch_kernel,
        out_shape=[pltpu.VMEM((capacity, width), bf16)] * line_n,
        in_specs=[vmem] * 3,
        out_specs=[vmem] * line_n,
        name="sent",
        compiler_params=pltpu.CompilerParams(vmem_limit_bytes=8 << 20),
    )(*in_vmem(picks, hidden, second_gain[None]))
    rows = [sent[0]] + [shifted(sent[by], "x", by) for by in range(1, line_n)]
    anywhere = pl.BlockSpec(memory_space=pl.ANY)
    hidden_units = expert_gate.shape[2]
    dense_term, own_row, gate_near, up_near = pl.pallas_call(
        dense_kernel,
        out_shape=(
            pltpu.VMEM((batch, width), f32),
            pltpu.VMEM((1, width), f32),
            pltpu.VMEM((width, hidden_units), bf16),
            pltpu.VMEM((width, hidden_units), bf16),
        ),
        in_specs=[smem] + [vmem] * (3 + line_n) + [anywhere] * 2,
        out_specs=(vmem,) * 4,
        scratch_shapes=[pltpu.SemaphoreType.DMA((2,))],
        name="dense_term",
        compiler_params=pltpu.CompilerParams(vmem_limit_bytes=12 << 20),
        cost_estimate=pl.CostEstimate(
            flops=8 * batch * block * width, transcendentals=0, bytes_accessed=4 * width * 448
        ),
    )(
        (seq_count * row_at + tp_at).reshape(1),
        *in_vmem(hidden, second_gain[None], dense_gate[None], *lines),
        *in_hbm(expert_gate, expert_up),
    )
    expert_rows = pl.pallas_call(
        expert_kernel,
        out_shape=[pltpu.VMEM((capacity, width), bf16)] * line_n,
        in_specs=[vmem] * (line_n + 2) + [anywhere],
        out_specs=[vmem] * line_n,
        scratch_shapes=[
            pltpu.VMEM((hidden_units, width), bf16),
            pltpu.SemaphoreType.DMA((2,)),
        ],
        name="expert",
        compiler_params=pltpu.CompilerParams(vmem_limit_bytes=20 << 20),
    )(*in_vmem(*rows, gate_near, up_near), *in_hbm(expert_down))
    returned = [expert_rows[0]] + [shifted(expert_rows[by], "x", -by) for by in range(1, line_n)]
    terms = pl.pallas_call(
        combine_kernel,
        out_shape=pltpu.VMEM((batch, width), bf16),
        in_specs=[vmem] * (2 + line_n),
        out_specs=vmem,
        name="terms",
        compiler_params=pltpu.CompilerParams(vmem_limit_bytes=8 << 20),
    )(*in_vmem(placed, dense_term, *returned))
    terms = exchanged(terms.reshape(rows_n, seq_count, width), ROW_AXES)
    sums = jnp.sum(terms.astype(f32), axis=0)
    other = jnp.where(tp_at == 0, sums[1:], sums[:1])
    mine = jnp.where(tp_at == 0, sums[:1], sums[1:])
    layer_out = (own_row + (mine + shifted(other, "tp", 1))).astype(bf16)
    return (layer_out, state_out, conv_out, conv_proj_out)


def solution(mesh):
    torus = Mesh(mesh.devices.reshape(8, 4, 4, mesh.shape["tp"]), EP_TP)
    return jax.shard_map(
        local,
        mesh=torus,
        in_specs=(
            P(EP, None),
            P(EP, "tp", None, None),
            P(EP, None, "tp"),
            P(EP, None, None, "tp"),
            P(),
            P(EP, "tp"),
            P(EP, "tp"),
            P(None, "tp"),
            P(None, "tp"),
            P(None, "tp"),
            P(None, "tp"),
            P(None, None, "tp"),
            P("tp"),
            P("tp"),
            P("tp"),
            P("tp"),
            P("tp", EP),
            P(),
            P(EP, None),
            P(EP, None),
            P(EP, None, "tp"),
            P(EP, None, "tp"),
            P(EP, "tp", None),
            P(None, EP_TP),
            P(EP_TP, None),
            P(),
        ),
        out_specs=(
            P(EP_TP, None),
            P(EP, "tp", None, None),
            P(EP, None, "tp"),
            P(EP, None, None, "tp"),
        ),
        check_vma=False,
    )
```

time: 145 us -> 129 us (0.89)
  other arithmetic: 15.5 us -> 5.33 us
  matrix products: 12.2 us -> 2.46 us
  Pallas kernels: 0 us -> 8.27 us
  local copies, waits for them, and re-layouts: 12.3 us -> 6.04 us
  starting transfers between devices: 48.6 us -> 52.1 us
    dot_general x7 -> x0, matrix products: 9.87 us -> none  [the longest x1 3.4 us: local(): jnp.dot(activated, expert_down[0], preferred_element_type=f32).astype(bf16)]
    pallas_call x0 -> x6, Pallas kernels: none -> 8.27 us  [the longest x1 2.96 us: local(): pl.pallas_call(dense_kernel, out_shape=(pltpu.VMEM((batch, width), f32),...]
    ppermute x10 -> x11, starting transfers between devices: 15.4 us -> 20.1 us  [shifted(): lax.ppermute(block, axis, [(i, (i + by) % size) for i in range(size)])]
    slice x3 -> x0, other arithmetic: 2.83 us -> none  [the longest x1 1.85 us: local(): line_up = lines[:, 2 * share:3 * share].reshape(block, width)]
    unnamed x43 -> x38, local copies, waits for them, and re-layouts: 4.23 us -> 1.64 us
    ppermute x10 -> x11, waiting for transfers between devices: 8.76 us -> 6.53 us  [shifted(): lax.ppermute(block, axis, [(i, (i + by) % size) for i in range(size)])]
    reduce_sum x4 -> x1, other arithmetic: 2.33 us -> 0.22 us  [local(): sums = jnp.sum(terms.astype(f32), axis=0)]
    slice x3 -> x0, local copies, waits for them, and re-layouts: 1.88 us -> none  [the longest x1 1.84 us: local(): expert_rows[0]]
  transfers between devices with their start and end apart: 15 -> 16, of which waited for: 11 -> 10; matrix products, arithmetic and copies ran while one was open for 10% -> 5% of each run, Pallas kernels for 0% -> 2%
where the time goes in v2:
time: 129 us
  waiting for transfers between devices  53.2 us (41%)
  starting transfers between devices  52.1 us (40%)
  Pallas kernels  8.27 us (6%)
  local copies, waits for them, and re-layouts  6.04 us (5%)
  other arithmetic  5.33 us (4%)
  matrix products  2.46 us (2%)
    all_to_all x5, waiting for transfers between devices, exchanged(): return lax.all_to_all(pieces, axis, split_axis=0, concat_axis=0, tiled=True)  46.7 us
    all_to_all x5, starting transfers between devices, exchanged(): return lax.all_to_all(pieces, axis, split_axis=0, concat_axis=0, tiled=True)  32.1 us
    ppermute x11, starting transfers between devices, shifted(): lax.ppermute(block, axis, [(i, (i + by) % size) for i in range(size)])  20.1 us
    ppermute x11, waiting for transfers between devices, shifted(): lax.ppermute(block, axis, [(i, (i + by) % size) for i in range(size)])  6.53 us
    pallas_call x1, Pallas kernels, local(): pl.pallas_call(dense_kernel, out_shape=(pltpu.VMEM((batch, width), f32),...  2.96 us
  transfers between devices with their start and end apart: 16, of which 10 were waited for; matrix products, arithmetic and copies ran while one was open for 5% of the time, Pallas kernels for 2%

profile of v2, /device:TPU:1, one launch (start us, length us, event | category | flops | bytes accessed | tf_op | source)
XLA Modules:
  0.0 128.6 jit_solution(11780434824546450817)
XLA Ops:
  0.7 1.9 %start.1 = (bf16[32,2,256]{2,1,0:T(2,128)(2,1)}, bf16[2,2048]{1,0:T(2,128)(2,1)S(1)}, bf16[56,2048]{1,0:T(8,128)(2,1)S(1)}) custom-call(bf16[2,2048]{1,0:T(2,128)(2,1)} %tokens.1, f32[1,2048]{1,0:T(1,128)} %bitcast.54, s32[2,4]{1,0:T(2,128)} %routes.1, bf16[2,4]{1,0:T(2,128)(2,1)} %logits.1, bf16[16,1024]{1,0:T(8,128)(2,1)} %gate_weight.1, ...), custom_call_target="tpu_custom_call" | custom-call | tf_op jit(solution)/shard_map/start/pallas_call | solution.py:295
  2.6 3.3 %collective-permute-start = (bf16[56,2048]{1,0:T(8,128)(2,1)S(1)}, bf16[56,2048]{1,0:T(8,128)(2,1)S(1)}, u32[]{:S(2)}, u32[]{:S(2)}) collective-permute-start(bf16[56,2048]{1,0:T(8,128)(2,1)S(1)} %get-tuple-element.20.h0), channel_id=1, source_target_pairs={{0,6},{2,0},{4,2},{6,4},{1,7},{3,1},{5,3},{7,5},{8,14},{10,8},{12,... | collective-permute-start | bytes 688136 | tf_op jit(solution)/shard_map/ppermute | solution.py:36
  7.0 11.2 %all-to-all-start = ((bf16[32,2,256]{2,1,0:T(2,128)(2,1)}), bf16[32,2,256]{2,1,0:T(2,128)(2,1)S(1)}, u32[]{:S(2)}, u32[]{:S(2)}) async-start(bf16[32,2,256]{2,1,0:T(2,128)(2,1)} %get-tuple-element.19), calls=%async_computation | async-start | bytes 65536 | tf_op jit(solution)/shard_map/all_to_all | solution.py:31
  19.1 1.6 %fusion.2 = bf16[2,1,256]{2,0,1:T(2,128)(2,1)S(1)} fusion(bf16[2,2048]{1,0:T(2,128)(2,1)S(1)} %get-tuple-element.21, bf16[2048,256]{1,0:T(8,128)(2,1)} %param.34), kind=kOutput, calls=%fused_computation.5 | convolution fusion | flops 2097664 | bytes 1057792 | tf_op jit(solution)/shard_map/dot_general | solution.py:354
  21.3 5.6 %all-to-all-done = bf16[32,2,256]{2,1,0:T(2,128)(2,1)S(1)} async-done(((bf16[32,2,256]{2,1,0:T(2,128)(2,1)}), bf16[32,2,256]{2,1,0:T(2,128)(2,1)S(1)}, u32[]{:S(2)}, u32[]{:S(2)}) %all-to-all-start) | async-done | bytes 32800 | tf_op jit(solution)/shard_map/all_to_all | solution.py:31
  26.9 0.7 slice_reduce_fusion
  28.1 0.9 reshape.129
  29.0 3.9 %all-to-all-start.1 = ((bf16[32,2,2048]{2,1,0:T(2,128)(2,1)}), bf16[32,2,2048]{2,1,0:T(2,128)(2,1)S(1)}, u32[]{:S(2)}, u32[]{:S(2)}) async-start(bf16[32,2,2048]{2,1,0:T(2,128)(2,1)} %reshape.129), calls=%async_computation.1 | async-start | bytes 524288 | tf_op jit(solution)/shard_map/all_to_all | solution.py:31
  32.9 10.5 %all-to-all-done.1 = bf16[32,2,2048]{2,1,0:T(2,128)(2,1)S(1)} async-done(((bf16[32,2,2048]{2,1,0:T(2,128)(2,1)}), bf16[32,2,2048]{2,1,0:T(2,128)(2,1)S(1)}, u32[]{:S(2)}, u32[]{:S(2)}) %all-to-all-start.1) | async-done | bytes 262176 | tf_op jit(solution)/shard_map/all_to_all | solution.py:31
  43.9 1.4 %multiply_reduce_fusion = (f32[2,16,64]{2,1,0:T(8,128)S(1)}, f32[2,16,64,128]{3,2,1,0:T(8,128)}) fusion(f32[2,16,128]{2,1,0:T(8,128)S(1)} %get-tuple-element.46, f32[2,16,128]{2,1,0:T(8,128)S(1)} %get-tuple-element.47, f32[2,16,64]{2,1,0:T(8,128)S(1)} %multiply_multiply_fusion, f32[2,16,64,128]{3,2,1,0:T(8,128)S(1)} %copy-done.3, ...), kind=kLoop, calls=%fused_computation.7 | loop fusion | flops 1308672 | bytes 2146432 | tf_op jit(solution)/shard_map/reduce_sum | solution.py:240
  45.6 0.7 broadcast_in_dim.82
  46.3 3.8 %all-to-all-start.2 = ((bf16[32,2,1024]{2,1,0:T(2,128)(2,1)}), bf16[32,2,1024]{2,1,0:T(2,128)(2,1)S(1)}, u32[]{:S(2)}, u32[]{:S(2)}) async-start(bf16[32,2,1024]{2,1,0:T(2,128)(2,1)} %broadcast_in_dim.82), calls=%async_computation.2 | async-start | bytes 262144 | tf_op jit(solution)/shard_map/all_to_all | solution.py:31
  50.2 9.4 %all-to-all-done.2 = bf16[32,2,1024]{2,1,0:T(2,128)(2,1)S(1)} async-done(((bf16[32,2,1024]{2,1,0:T(2,128)(2,1)}), bf16[32,2,1024]{2,1,0:T(2,128)(2,1)S(1)}, u32[]{:S(2)}, u32[]{:S(2)}) %all-to-all-start.2) | async-done | bytes 131104 | tf_op jit(solution)/shard_map/all_to_all | solution.py:31
  60.1 5.2 %collective-permute-start.3 = (f32[64,64]{0,1:T(8,128)S(1)}, f32[64,64]{0,1:T(8,128)S(1)}, u32[]{:S(2)}, u32[]{:S(2)}) collective-permute-start(f32[64,64]{0,1:T(8,128)S(1)} %fusion), channel_id=1, source_target_pairs={{0,1},{1,0},{2,3},{3,2},{4,5},{5,4},{6,7},{7,6},{8,9},{9,8},{10,11... | collective-permute-start | bytes 49160 | tf_op jit(solution)/shard_map/ppermute | solution.py:36
  65.4 0.8 collective-permute-done.3
  66.4 1.1 reshape.133
  67.5 3.9 %all-to-all-start.3 = ((bf16[32,2,2048]{2,1,0:T(2,128)(2,1)}), bf16[32,2,2048]{2,1,0:T(2,128)(2,1)S(1)}, u32[]{:S(2)}, u32[]{:S(2)}) async-start(bf16[32,2,2048]{2,1,0:T(2,128)(2,1)} %reshape.133), calls=%async_computation.3 | async-start | bytes 524288 | tf_op jit(solution)/shard_map/all_to_all | solution.py:31
  72.1 11.1 %all-to-all-done.3 = bf16[32,2,2048]{2,1,0:T(2,128)(2,1)S(1)} async-done(((bf16[32,2,2048]{2,1,0:T(2,128)(2,1)}), bf16[32,2,2048]{2,1,0:T(2,128)(2,1)S(1)}, u32[]{:S(2)}, u32[]{:S(2)}) %all-to-all-start.3) | async-done | bytes 262176 | tf_op jit(solution)/shard_map/all_to_all | solution.py:31
  84.1 1.6 %collective-permute-start.4 = (bf16[32,2048]{1,0:T(8,128)(2,1)S(1)}, bf16[32,2048]{1,0:T(8,128)(2,1)S(1)}, u32[]{:S(2)}, u32[]{:S(2)}) collective-permute-start(bf16[32,2048]{1,0:T(8,128)(2,1)S(1)} %get-tuple-element.25), channel_id=1, source_target_pairs={{0,2},{2,4},{4,6},{6,0},{1,3},{3,5},{5,7},{7,1},{8,10},{10,12},{12... | collective-permute-start | bytes 393224 | tf_op jit(solution)/shard_map/ppermute | solution.py:36
  85.7 1.7 %collective-permute-start.5 = (bf16[32,2048]{1,0:T(8,128)(2,1)S(1)}, bf16[32,2048]{1,0:T(8,128)(2,1)S(1)}, u32[]{:S(2)}, u32[]{:S(2)}) collective-permute-start(bf16[32,2048]{1,0:T(8,128)(2,1)S(1)} %get-tuple-element.26), channel_id=1, source_target_pairs={{0,4},{2,6},{4,0},{6,2},{1,5},{3,7},{5,1},{7,3},{8,12},{10,14},{12... | collective-permute-start | bytes 393224 | tf_op jit(solution)/shard_map/ppermute | solution.py:36
  87.4 0.8 collective-permute-start.6
  88.5 3.0 %dense_term.1 = (f32[64,2048]{1,0:T(8,128)S(1)}, f32[1,2048]{1,0:T(1,128)S(1)}, bf16[2048,512]{1,0:T(8,128)(2,1)S(1)}, bf16[2048,512]{1,0:T(8,128)(2,1)S(1)}) custom-call(s32[1]{0:T(128)} %bitcast.own_at, bf16[2048,64]{1,0:T(8,128)(2,1)S(1)} %bitcast.44, f32[1,2048]{1,0:T(1,128)S(1)} %bitcast.46, f32[1,2048]{1,0:T(1,128)S(1)} %bitcast.47, ...), custom_call_target="tpu_custom_call" | custom-call | flops 67108864 | bytes 3670016 | tf_op jit(solution)/shard_map/dense_term/pallas_call | solution.py:409
  91.6 2.4 %expert.1 = (bf16[32,2048]{1,0:T(8,128)(2,1)S(1)}, bf16[32,2048]{1,0:T(8,128)(2,1)S(1)}, bf16[32,2048]{1,0:T(8,128)(2,1)S(1)}, bf16[32,2048]{1,0:T(8,128)(2,1)S(1)}) custom-call(bf16[32,2048]{1,0:T(8,128)(2,1)S(1)} %get-tuple-element.24.own, bf16[32,2048]{1,0:T(8,128)(2,1)S(1)} %collective-permute-done.4.one, ...), custom_call_target="tpu_custom_call" | custom-call | tf_op jit(solution)/shard_map/expert/pallas_call | solution.py:430
  94.0 2.1 %collective-permute-start.7 = (bf16[32,2048]{1,0:T(8,128)(2,1)S(1)}, bf16[32,2048]{1,0:T(8,128)(2,1)S(1)}, u32[]{:S(2)}, u32[]{:S(2)}) collective-permute-start(bf16[32,2048]{1,0:T(8,128)(2,1)S(1)} %get-tuple-element.31), channel_id=1, source_target_pairs={{0,6},{2,0},{4,2},{6,4},{1,7},{3,1},{5,3},{7,5},{8,14},{10,8},{12,... | collective-permute-start | bytes 393224 | tf_op jit(solution)/shard_map/ppermute | solution.py:36
  96.1 1.2 collective-permute-start.8
  97.3 2.1 %collective-permute-done.7.e1 = bf16[32,2048]{1,0:T(8,128)(2,1)S(1)} collective-permute-done((bf16[32,2048]{1,0:T(8,128)(2,1)S(1)}, bf16[32,2048]{1,0:T(8,128)(2,1)S(1)}, u32[]{:S(2)}, u32[]{:S(2)}) %collective-permute-start.7) | collective-permute-done | bytes 131104 | tf_op jit(solution)/shard_map/ppermute | solution.py:36
  99.4 2.1 %collective-permute-done.8.e2 = bf16[32,2048]{1,0:T(8,128)(2,1)S(1)} collective-permute-done((bf16[32,2048]{1,0:T(8,128)(2,1)S(1)}, bf16[32,2048]{1,0:T(8,128)(2,1)S(1)}, u32[]{:S(2)}, u32[]{:S(2)}) %collective-permute-start.8) | collective-permute-done | bytes 131104 | tf_op jit(solution)/shard_map/ppermute | solution.py:36
  101.4 1.4 %collective-permute-done.9.e3 = bf16[32,2048]{1,0:T(8,128)(2,1)S(1)} collective-permute-done((bf16[32,2048]{1,0:T(8,128)(2,1)S(1)}, bf16[32,2048]{1,0:T(8,128)(2,1)S(1)}, u32[]{:S(2)}, u32[]{:S(2)}) %collective-permute-start.9) | collective-permute-done | bytes 131104 | tf_op jit(solution)/shard_map/ppermute | solution.py:36
  103.0 0.9 reshape.132
  103.9 9.3 %all-to-all-start.4 = ((bf16[32,2,2048]{2,1,0:T(2,128)(2,1)}), bf16[32,2,2048]{2,1,0:T(2,128)(2,1)S(1)}, u32[]{:S(2)}, u32[]{:S(2)}) async-start(bf16[32,2,2048]{2,1,0:T(2,128)(2,1)} %reshape.132), calls=%async_computation.4 | async-start | bytes 524288 | tf_op jit(solution)/shard_map/all_to_all | solution.py:31
  113.8 10.0 %all-to-all-done.4 = bf16[32,2,2048]{2,1,0:T(2,128)(2,1)S(1)} async-done(((bf16[32,2,2048]{2,1,0:T(2,128)(2,1)}), bf16[32,2,2048]{2,1,0:T(2,128)(2,1)S(1)}, u32[]{:S(2)}, u32[]{:S(2)}) %all-to-all-start.4) | async-done | bytes 262176 | tf_op jit(solution)/shard_map/all_to_all | solution.py:31
  124.1 3.1 %collective-permute-start.10 = (f32[1,2048]{1,0:T(1,128)S(1)}, f32[1,2048]{1,0:T(1,128)S(1)}, u32[]{:S(2)}, u32[]{:S(2)}) collective-permute-start(f32[1,2048]{1,0:T(1,128)S(1)} %broadcast_select_fusion), channel_id=1, source_target_pairs={{0,1},{1,0},{2,3},{3,2},{4,5},{5,4},{6,7},{7,6},{8,9},{9,8},{10,11... | collective-permute-start | bytes 24584 | tf_op jit(solution)/shard_map/ppermute | solution.py:36
  (105 shorter events, 9.0 us)
Async XLA Ops:
  0.6 18.2 %copy-start = (bf16[2048,256]{1,0:T(8,128)(2,1)S(1)}, bf16[2048,256]{1,0:T(8,128)(2,1)}, u32[]{:S(2)}) copy-start(bf16[2048,256]{1,0:T(8,128)(2,1)} %param.33) | copy-start | bytes 3145732
  0.7 20.1 %copy-start.7 = (bf16[2,3,2,256]{3,2,1,0:T(2,128)(2,1)S(1)}, bf16[2,3,2,256]{3,2,1,0:T(2,128)(2,1)}, u32[]{:S(2)}) copy-start(bf16[2,3,2,256]{3,2,1,0:T(2,128)(2,1)} %param.29) | copy-start | bytes 18436
  0.7 20.1 %copy-start.6 = (f32[4,2,256]{2,1,0:T(2,128)S(1)}, f32[4,2,256]{2,1,0:T(2,128)}, u32[]{:S(2)}) copy-start(f32[4,2,256]{2,1,0:T(2,128)} %param.37) | copy-start | bytes 24580
  0.7 20.2 %copy-start.11 = (bf16[2048,16]{0,1:T(8,128)(2,1)S(1)}, bf16[2048,16]{0,1:T(8,128)(2,1)}, u32[]{:S(2)}) copy-start(bf16[2048,16]{0,1:T(8,128)(2,1)} %param.35) | copy-start | bytes 196612
  0.7 20.2 %copy-start.12 = (f32[16]{0:T(128)S(1)}, f32[16]{0:T(128)}, u32[]{:S(2)}) copy-start(f32[16]{0:T(128)} %param.38) | copy-start | bytes 196
  0.7 20.4 %copy-start.10 = (f32[16]{0:T(128)S(1)}, f32[16]{0:T(128)}, u32[]{:S(2)}) copy-start(f32[16]{0:T(128)} %param.40) | copy-start | bytes 196
  2.6 25.1 %collective-permute-start = (bf16[56,2048]{1,0:T(8,128)(2,1)S(1)}, bf16[56,2048]{1,0:T(8,128)(2,1)S(1)}, u32[]{:S(2)}, u32[]{:S(2)}) collective-permute-start(bf16[56,2048]{1,0:T(8,128)(2,1)S(1)} %get-tuple-element.20.h0), channel_id=1, source_target_pairs={{0,6},{2,0},{4,2},{6,4},{1,7},{3,1},{5,3},{7,5},{8,14},{10,8},{12,... | collective-permute-start | bytes 688136 | tf_op jit(solution)/shard_map/ppermute | solution.py:36
  5.9 21.8 %collective-permute-start.1 = (bf16[56,2048]{1,0:T(8,128)(2,1)S(1)}, bf16[56,2048]{1,0:T(8,128)(2,1)S(1)}, u32[]{:S(2)}, u32[]{:S(2)}) collective-permute-start(bf16[56,2048]{1,0:T(8,128)(2,1)S(1)} %get-tuple-element.20.h0), channel_id=1, source_target_pairs={{0,4},{2,6},{4,0},{6,2},{1,5},{3,7},{5,1},{7,3},{8,12},{10,14},{12... | collective-permute-start | bytes 688136 | tf_op jit(solution)/shard_map/ppermute | solution.py:36
  6.4 21.3 %collective-permute-start.2 = (bf16[56,2048]{1,0:T(8,128)(2,1)S(1)}, bf16[56,2048]{1,0:T(8,128)(2,1)S(1)}, u32[]{:S(2)}, u32[]{:S(2)}) collective-permute-start(bf16[56,2048]{1,0:T(8,128)(2,1)S(1)} %get-tuple-element.20.h0), channel_id=1, source_target_pairs={{0,2},{2,4},{4,6},{6,0},{1,3},{3,5},{5,7},{7,1},{8,10},{10,12},{12... | collective-permute-start | bytes 688136 | tf_op jit(solution)/shard_map/ppermute | solution.py:36
  7.0 19.9 %all-to-all-start = ((bf16[32,2,256]{2,1,0:T(2,128)(2,1)}), bf16[32,2,256]{2,1,0:T(2,128)(2,1)S(1)}, u32[]{:S(2)}, u32[]{:S(2)}) async-start(bf16[32,2,256]{2,1,0:T(2,128)(2,1)} %get-tuple-element.19), calls=%async_computation | async-start | bytes 65536 | tf_op jit(solution)/shard_map/all_to_all | solution.py:31
  19.1 24.5 %copy-start.4 = (bf16[2,3,1024]{2,0,1:T(2,128)(2,1)S(1)}, bf16[2,3,1024]{2,0,1:T(2,128)(2,1)}, u32[]{:S(2)}) copy-start(bf16[2,3,1024]{2,0,1:T(2,128)(2,1)} %param.28) | copy-start | bytes 36868
  19.1 24.5 %copy-start.5 = (f32[4,1024]{1,0:T(4,128)S(1)}, f32[4,1024]{1,0:T(4,128)}, u32[]{:S(2)}) copy-start(f32[4,1024]{1,0:T(4,128)} %param.36) | copy-start | bytes 49156
  19.1 24.7 %copy-start.3 = (f32[2,16,64,128]{3,2,1,0:T(8,128)S(1)}, f32[2,16,64,128]{3,2,1,0:T(8,128)}, u32[]{:S(2)}) copy-start(f32[2,16,64,128]{3,2,1,0:T(8,128)} %param.27) | copy-start | bytes 3145732
  28.1 17.5 %copy-start.8 = (f32[1024]{0:T(1024)S(1)}, f32[1024]{0:T(1024)}, u32[]{:S(2)}) copy-start(f32[1024]{0:T(1024)} %param.41) | copy-start | bytes 12292
  29.0 14.5 %all-to-all-start.1 = ((bf16[32,2,2048]{2,1,0:T(2,128)(2,1)}), bf16[32,2,2048]{2,1,0:T(2,128)(2,1)S(1)}, u32[]{:S(2)}, u32[]{:S(2)}) async-start(bf16[32,2,2048]{2,1,0:T(2,128)(2,1)} %reshape.129), calls=%async_computation.1 | async-start | bytes 524288 | tf_op jit(solution)/shard_map/all_to_all | solution.py:31
  45.2 26.6 %copy-start.9 = (bf16[64]{0:T(256)(128)(2,1)S(1)}, bf16[64]{0:T(256)(128)(2,1)}, u32[]{:S(2)}) copy-start(bf16[64]{0:T(256)(128)(2,1)} %get-tuple-element.40) | copy-start | bytes 388
  45.6 38.0 %copy-start.1 = (f32[2048]{0:T(1024)S(1)}, f32[2048]{0:T(1024)}, u32[]{:S(2)}) copy-start(f32[2048]{0:T(1024)} %param.43) | copy-start | bytes 24580
  46.3 13.3 %all-to-all-start.2 = ((bf16[32,2,1024]{2,1,0:T(2,128)(2,1)}), bf16[32,2,1024]{2,1,0:T(2,128)(2,1)S(1)}, u32[]{:S(2)}, u32[]{:S(2)}) async-start(bf16[32,2,1024]{2,1,0:T(2,128)(2,1)} %broadcast_in_dim.82), calls=%async_computation.2 | async-start | bytes 262144 | tf_op jit(solution)/shard_map/all_to_all | solution.py:31
  59.6 28.9 %copy-start.2 = (f32[2048]{0:T(1024)S(1)}, f32[2048]{0:T(1024)}, u32[]{:S(2)}) copy-start(f32[2048]{0:T(1024)} %param.51) | copy-start | bytes 24580
  60.1 6.1 %collective-permute-start.3 = (f32[64,64]{0,1:T(8,128)S(1)}, f32[64,64]{0,1:T(8,128)S(1)}, u32[]{:S(2)}, u32[]{:S(2)}) collective-permute-start(f32[64,64]{0,1:T(8,128)S(1)} %fusion), channel_id=1, source_target_pairs={{0,1},{1,0},{2,3},{3,2},{4,5},{5,4},{6,7},{7,6},{8,9},{9,8},{10,11... | collective-permute-start | bytes 49160 | tf_op jit(solution)/shard_map/ppermute | solution.py:36
  67.5 15.7 %all-to-all-start.3 = ((bf16[32,2,2048]{2,1,0:T(2,128)(2,1)}), bf16[32,2,2048]{2,1,0:T(2,128)(2,1)S(1)}, u32[]{:S(2)}, u32[]{:S(2)}) async-start(bf16[32,2,2048]{2,1,0:T(2,128)(2,1)} %reshape.133), calls=%async_computation.3 | async-start | bytes 524288 | tf_op jit(solution)/shard_map/all_to_all | solution.py:31
  84.1 7.5 %collective-permute-start.4 = (bf16[32,2048]{1,0:T(8,128)(2,1)S(1)}, bf16[32,2048]{1,0:T(8,128)(2,1)S(1)}, u32[]{:S(2)}, u32[]{:S(2)}) collective-permute-start(bf16[32,2048]{1,0:T(8,128)(2,1)S(1)} %get-tuple-element.25), channel_id=1, source_target_pairs={{0,2},{2,4},{4,6},{6,0},{1,3},{3,5},{5,7},{7,1},{8,10},{10,12},{12... | collective-permute-start | bytes 393224 | tf_op jit(solution)/shard_map/ppermute | solution.py:36
  85.7 5.9 %collective-permute-start.5 = (bf16[32,2048]{1,0:T(8,128)(2,1)S(1)}, bf16[32,2048]{1,0:T(8,128)(2,1)S(1)}, u32[]{:S(2)}, u32[]{:S(2)}) collective-permute-start(bf16[32,2048]{1,0:T(8,128)(2,1)S(1)} %get-tuple-element.26), channel_id=1, source_target_pairs={{0,4},{2,6},{4,0},{6,2},{1,5},{3,7},{5,1},{7,3},{8,12},{10,14},{12... | collective-permute-start | bytes 393224 | tf_op jit(solution)/shard_map/ppermute | solution.py:36
  87.4 4.2 %collective-permute-start.6 = (bf16[32,2048]{1,0:T(8,128)(2,1)S(1)}, bf16[32,2048]{1,0:T(8,128)(2,1)S(1)}, u32[]{:S(2)}, u32[]{:S(2)}) collective-permute-start(bf16[32,2048]{1,0:T(8,128)(2,1)S(1)} %get-tuple-element.27), channel_id=1, source_target_pairs={{0,6},{2,0},{4,2},{6,4},{1,7},{3,1},{5,3},{7,5},{8,14},{10,8},{12,... | collective-permute-start | bytes 393224 | tf_op jit(solution)/shard_map/ppermute | solution.py:36
  94.0 5.4 %collective-permute-start.7 = (bf16[32,2048]{1,0:T(8,128)(2,1)S(1)}, bf16[32,2048]{1,0:T(8,128)(2,1)S(1)}, u32[]{:S(2)}, u32[]{:S(2)}) collective-permute-start(bf16[32,2048]{1,0:T(8,128)(2,1)S(1)} %get-tuple-element.31), channel_id=1, source_target_pairs={{0,6},{2,0},{4,2},{6,4},{1,7},{3,1},{5,3},{7,5},{8,14},{10,8},{12,... | collective-permute-start | bytes 393224 | tf_op jit(solution)/shard_map/ppermute | solution.py:36
  96.1 5.4 %collective-permute-start.8 = (bf16[32,2048]{1,0:T(8,128)(2,1)S(1)}, bf16[32,2048]{1,0:T(8,128)(2,1)S(1)}, u32[]{:S(2)}, u32[]{:S(2)}) collective-permute-start(bf16[32,2048]{1,0:T(8,128)(2,1)S(1)} %get-tuple-element.32), channel_id=1, source_target_pairs={{0,4},{2,6},{4,0},{6,2},{1,5},{3,7},{5,1},{7,3},{8,12},{10,14},{12... | collective-permute-start | bytes 393224 | tf_op jit(solution)/shard_map/ppermute | solution.py:36
  97.3 5.5 %collective-permute-start.9 = (bf16[32,2048]{1,0:T(8,128)(2,1)S(1)}, bf16[32,2048]{1,0:T(8,128)(2,1)S(1)}, u32[]{:S(2)}, u32[]{:S(2)}) collective-permute-start(bf16[32,2048]{1,0:T(8,128)(2,1)S(1)} %get-tuple-element.33), channel_id=1, source_target_pairs={{0,2},{2,4},{4,6},{6,0},{1,3},{3,5},{5,7},{7,1},{8,10},{10,12},{12... | collective-permute-start | bytes 393224 | tf_op jit(solution)/shard_map/ppermute | solution.py:36
  103.9 19.9 %all-to-all-start.4 = ((bf16[32,2,2048]{2,1,0:T(2,128)(2,1)}), bf16[32,2,2048]{2,1,0:T(2,128)(2,1)S(1)}, u32[]{:S(2)}, u32[]{:S(2)}) async-start(bf16[32,2,2048]{2,1,0:T(2,128)(2,1)} %reshape.132), calls=%async_computation.4 | async-start | bytes 524288 | tf_op jit(solution)/shard_map/all_to_all | solution.py:31
  124.1 3.9 %collective-permute-start.10 = (f32[1,2048]{1,0:T(1,128)S(1)}, f32[1,2048]{1,0:T(1,128)S(1)}, u32[]{:S(2)}, u32[]{:S(2)}) collective-permute-start(f32[1,2048]{1,0:T(1,128)S(1)} %broadcast_select_fusion), channel_id=1, source_target_pairs={{0,1},{1,0},{2,3},{3,2},{4,5},{5,4},{6,7},{7,6},{8,9},{9,8},{10,11... | collective-permute-start | bytes 24584 | tf_op jit(solution)/shard_map/ppermute | solution.py:36

commit v3 on v2

--- a/solution.py
+++ b/solution.py
@@ -105,9 +105,53 @@
     part[...] = jnp.dot(turned, weight, preferred_element_type=f32).astype(bf16)
 
 
-def dispatch_kernel(picks, hidden, gain, r0, r1, r2, r3):
+def out_kernel(line_at, mixer, h0, h1, h2, h3, part):
+    share = h0.shape[0] // 7 * 2
+    block, channels = part.shape[0], mixer.shape[1]
+    row = lax.broadcasted_iota(jnp.int32, (block, block), 0)
+    column = lax.broadcasted_iota(jnp.int32, (block, block), 1)
+    turn = (column == (row + block - share * line_at[0]) % block).astype(bf16)
+    weight = jnp.concatenate(
+        [
+            h[3 * share :, at : at + channels].astype(f32)
+            for h in (h0, h1, h2, h3)
+            for at in (0, channels)
+        ],
+        axis=0,
+    ).astype(bf16)
+    weight = jnp.dot(turn, weight, preferred_element_type=f32).astype(bf16)
+    part[...] = lax.dot_general(
+        weight, mixer[...], (((1,), (1,)), ((), ())), preferred_element_type=f32
+    )
+
+
+def hidden_kernel(part, other, spread, pieces):
+    block, _ = part.shape
+    row = lax.broadcasted_iota(jnp.int32, (block, 2 * block), 0)
+    column = lax.broadcasted_iota(jnp.int32, (block, 2 * block), 1)
+    raw = lax.dot_general(
+        (column == row + block).astype(bf16),
+        spread[:, : 2 * block],
+        (((1,), (1,)), ((), ())),
+        preferred_element_type=f32,
+    )
+    hidden = raw + (part[...] + other[...])
+    half = block // 2
+    packed = jnp.concatenate([hidden[:half], hidden[half:]], axis=1).astype(bf16)
+    pieces[...] = jnp.broadcast_to(packed[None], pieces.shape)
+
+
+def unpacked(pieces):
+    count, half, lanes = pieces.shape
+    low = pieces[...]
+    flat = low.reshape(count * half, lanes).astype(f32)
+    high = pltpu.roll(flat, lanes // 2, 1).astype(bf16).reshape(count, half, lanes)
+    return jnp.concatenate([low, high], axis=1).reshape(2 * count * half, lanes)
+
+
+def dispatch_kernel(picks, pieces, gain, r0, r1, r2, r3):
     rows = lax.dot_general(
-        picks[...], hidden[...], (((1,), (1,)), ((), ())), preferred_element_type=f32
+        picks[...], unpacked(pieces), (((1,), (1,)), ((), ())), preferred_element_type=f32
     )
     rows = rms_scale(rows, gain[...]).astype(bf16)
     count = r0.shape[0]
@@ -117,7 +161,7 @@
 
 def dense_kernel(
     own_at,
-    hidden,
+    pieces,
     gain,
     dense_gate,
     h0,
@@ -139,12 +183,12 @@
     for copy in copies:
         copy.start()
     share = h0.shape[0] // 7 * 2
-    batch = hidden.shape[1]
-    row = lax.broadcasted_iota(jnp.int32, (batch, batch), 0)
-    column = lax.broadcasted_iota(jnp.int32, (batch, batch), 1)
+    batch = term.shape[0]
+    row = lax.broadcasted_iota(jnp.int32, (batch, 2 * batch), 0)
+    column = lax.broadcasted_iota(jnp.int32, (batch, 2 * batch), 1)
     rows = lax.dot_general(
         (row == column).astype(bf16),
-        hidden[...],
+        unpacked(pieces),
         (((1,), (1,)), ((), ())),
         preferred_element_type=f32,
     )
@@ -232,18 +276,18 @@
     )
     step_size = jax.nn.softplus(step_raw + step_bias)
     decay_rate = jnp.exp(-jnp.exp(log_rate) * step_size)
-    state_out = (
-        decay_rate[:, :, None, None] * head_state
-        + (step_size[:, :, None] * head_input)[:, :, :, None] * write_heads[:, :, None, :]
-    )
-    read_out = (
-        jnp.sum(state_out * read_heads[:, :, None, :], axis=-1)
-        + skip_gain[None, :, None] * head_input
-    )
+    old_read = jnp.sum(head_state * read_heads[:, :, None, :], axis=-1) * decay_rate[:, :, None]
+    direct = step_size * jnp.sum(write_heads * read_heads, axis=-1) + skip_gain
+    read_out = old_read + direct[:, :, None] * head_input
     gated_rows = read_out.reshape(seq_count, channels) * jax.nn.silu(gate_proj.astype(f32))
     grouped = gated_rows.reshape(seq_count, group_count, channels // group_count)
     grouped = grouped * lax.rsqrt(jnp.mean(grouped * grouped, axis=-1, keepdims=True) + norm_eps)
     mixer_rows = (grouped.reshape(seq_count, channels) * group_gain).astype(bf16)
+    mixer_rows, head_state = lax.optimization_barrier((mixer_rows, head_state))
+    state_out = (
+        decay_rate[:, :, None, None] * head_state
+        + (step_size[:, :, None] * head_input)[:, :, :, None] * write_heads[:, :, None, :]
+    )
     return (mixer_rows, state_out, window_inner[:, 1:], window_proj[:, 1:])
 
 
@@ -317,28 +361,10 @@
     )
     spread = exchanged(features, ROW_AXES)
     spread = spread.reshape(batch, lanes)
-    raw_block = spread[:, block : 2 * block]
     all_routes = spread[:, 2 * block : 2 * block + topk]
     all_logits = spread[:, 2 * block + topk : 2 * block + 2 * topk].astype(f32)
 
     lines = [held] + [shifted(held, "x", -by) for by in range(1, line_n)]
-    order = jnp.arange(block, dtype=jnp.int32)
-    unturn = ((order[:, None] - share * line_at) % block == order[None, :]).astype(bf16)
-
-    def natural(part):
-        return jnp.dot(unturn, part, preferred_element_type=f32).astype(bf16)
-
-    line_out = natural(
-        jnp.concatenate(
-            [
-                part[3 * share :, at : at + channels]
-                for part in lines
-                for at in (0, channels)
-            ],
-            axis=0,
-        )
-    )
-
     in_part = pl.pallas_call(
         in_kernel,
         out_shape=pltpu.VMEM((batch, width), bf16),
@@ -373,14 +399,24 @@
     mixer_all = exchanged(
         jnp.broadcast_to(mixer_rows, (rows_n, seq_count, channels)), ROW_AXES
     ).reshape(batch, channels)
-    mixed_part = lax.dot_general(
-        line_out, mixer_all, (((1,), (1,)), ((), ())), preferred_element_type=f32
-    )
-    mixed = mixed_part + shifted(mixed_part, "tp", 1)
-    hidden_block = (raw_block.T.astype(f32) + mixed).astype(bf16)
-    hidden = exchanged(
-        jnp.broadcast_to(hidden_block, (rows_n, block, batch)), ROW_AXES
-    ).reshape(width, batch)
+    mixed_part = pl.pallas_call(
+        out_kernel,
+        out_shape=pltpu.VMEM((block, batch), f32),
+        in_specs=[smem] + [vmem] * (1 + line_n),
+        out_specs=vmem,
+        name="out_part",
+        compiler_params=pltpu.CompilerParams(vmem_limit_bytes=8 << 20),
+    )(line_at.reshape(1), *in_vmem(mixer_all, *lines))
+    other_part = shifted(mixed_part, "tp", 1)
+    pieces = pl.pallas_call(
+        hidden_kernel,
+        out_shape=jax.ShapeDtypeStruct((rows_n, block // 2, 2 * batch), bf16),
+        in_specs=[vmem] * 3,
+        out_specs=vmem,
+        name="hidden_pieces",
+        compiler_params=pltpu.CompilerParams(vmem_limit_bytes=8 << 20),
+    )(*in_vmem(mixed_part, other_part, spread))
+    hidden = exchanged(pieces, ROW_AXES)
 
     route_gates = jax.nn.softmax(all_logits, axis=-1)
     experts = (line_n * row_at + (line_at + jnp.arange(line_n)) % line_n).astype(bf16)
@@ -392,7 +428,9 @@
     slot_ids = jnp.arange(capacity, dtype=f32)
     picks = (slot[:, None, :] == slot_ids[None, :, None]) & chosen[:, None, :]
     placed = jnp.where(picks, row_weight[:, None, :], 0.0).astype(bf16)
-    picks = picks.astype(bf16).reshape(line_n * capacity, batch)
+    picks = jnp.pad(
+        picks.astype(bf16).reshape(line_n * capacity, batch), ((0, 0), (0, batch))
+    )
     placed = placed.reshape(line_n * capacity, batch).T
 
     sent = pl.pallas_call(

time: 129 us -> 126 us (0.977)
  waiting for transfers between devices: 53.2 us -> 50.5 us
  local copies, waits for them, and re-layouts: 6.04 us -> 4.51 us
  Pallas kernels: 8.27 us -> 9.66 us
    all_to_all x5, waiting for transfers between devices: 46.7 us -> 43.7 us  [exchanged(): return lax.all_to_all(pieces, axis, split_axis=0, concat_axis=0, tiled=True)]
    add x0 -> x1, other arithmetic: none -> 2.6 us  [state_step(): decay_rate[:, :, None, None] * head_state]
    unnamed x38 -> x29, local copies, waits for them, and re-layouts: 1.64 us -> 0.16 us
  transfers between devices with their start and end apart: 16 -> 16, of which waited for: 10 -> 12; matrix products, arithmetic and copies ran while one was open for 5% -> 7% of each run, Pallas kernels for 2% -> 2%
where the time goes in v3:
time: 126 us
  starting transfers between devices  52.1 us (41%)
  waiting for transfers between devices  50.5 us (40%)
  Pallas kernels  9.66 us (8%)
  other arithmetic  5.79 us (5%)
  local copies, waits for them, and re-layouts  4.51 us (4%)
  matrix products  1.99 us (2%)
    all_to_all x5, waiting for transfers between devices, exchanged(): return lax.all_to_all(pieces, axis, split_axis=0, concat_axis=0, tiled=True)  43.7 us
    all_to_all x5, starting transfers between devices, exchanged(): return lax.all_to_all(pieces, axis, split_axis=0, concat_axis=0, tiled=True)  32.5 us
    ppermute x11, starting transfers between devices, shifted(): lax.ppermute(block, axis, [(i, (i + by) % size) for i in range(size)])  19.6 us
    ppermute x11, waiting for transfers between devices, shifted(): lax.ppermute(block, axis, [(i, (i + by) % size) for i in range(size)])  6.77 us
    pallas_call x1, Pallas kernels, local(): pl.pallas_call(dense_kernel, out_shape=(pltpu.VMEM((batch, width), f32),...  3.02 us
    add x1, other arithmetic, state_step(): decay_rate[:, :, None, None] * head_state  2.6 us
  transfers between devices with their start and end apart: 16, of which 12 were waited for; matrix products, arithmetic and copies ran while one was open for 7% of the time, Pallas kernels for 2%

profile of v3, /device:TPU:1, one launch (start us, length us, event | category | flops | bytes accessed | tf_op | source)
XLA Modules:
  0.0 125.7 jit_solution(9192040936605408047)
XLA Ops:
  0.7 1.9 %start.1 = (bf16[32,2,256]{2,1,0:T(2,128)(2,1)}, bf16[2,2048]{1,0:T(2,128)(2,1)S(1)}, bf16[56,2048]{1,0:T(8,128)(2,1)S(1)}) custom-call(bf16[2,2048]{1,0:T(2,128)(2,1)} %tokens.1, f32[1,2048]{1,0:T(1,128)} %bitcast.49, s32[2,4]{1,0:T(2,128)} %routes.1, bf16[2,4]{1,0:T(2,128)(2,1)} %logits.1, bf16[16,1024]{1,0:T(8,128)(2,1)} %gate_weight.1, ...), custom_call_target="tpu_custom_call" | custom-call | tf_op jit(solution)/shard_map/start/pallas_call | solution.py:339
  2.6 3.3 %collective-permute-start = (bf16[56,2048]{1,0:T(8,128)(2,1)S(1)}, bf16[56,2048]{1,0:T(8,128)(2,1)S(1)}, u32[]{:S(2)}, u32[]{:S(2)}) collective-permute-start(bf16[56,2048]{1,0:T(8,128)(2,1)S(1)} %get-tuple-element.23.h0), channel_id=1, source_target_pairs={{0,6},{2,0},{4,2},{6,4},{1,7},{3,1},{5,3},{7,5},{8,14},{10,8},{12,... | collective-permute-start | bytes 688136 | tf_op jit(solution)/shard_map/ppermute | solution.py:36
  7.0 11.2 %all-to-all-start = ((bf16[32,2,256]{2,1,0:T(2,128)(2,1)}), bf16[32,2,256]{2,1,0:T(2,128)(2,1)S(1)}, u32[]{:S(2)}, u32[]{:S(2)}) async-start(bf16[32,2,256]{2,1,0:T(2,128)(2,1)} %get-tuple-element.22), calls=%async_computation | async-start | bytes 65536 | tf_op jit(solution)/shard_map/all_to_all | solution.py:31
  18.5 1.5 %fusion.1 = bf16[2,1,256]{2,0,1:T(2,128)(2,1)S(1)} fusion(bf16[2,2048]{1,0:T(2,128)(2,1)S(1)} %get-tuple-element.21, bf16[2048,256]{1,0:T(8,128)(2,1)} %param.34), kind=kOutput, calls=%fused_computation.3 | convolution fusion | flops 2097664 | bytes 1057792 | tf_op jit(solution)/shard_map/dot_general | solution.py:380
  20.9 6.0 %all-to-all-done = bf16[32,2,256]{2,1,0:T(2,128)(2,1)S(1)} async-done(((bf16[32,2,256]{2,1,0:T(2,128)(2,1)}), bf16[32,2,256]{2,1,0:T(2,128)(2,1)S(1)}, u32[]{:S(2)}, u32[]{:S(2)}) %all-to-all-start) | async-done | bytes 32800 | tf_op jit(solution)/shard_map/all_to_all | solution.py:31
  27.3 0.9 reshape.112
  28.2 4.2 %all-to-all-start.1 = ((bf16[32,2,2048]{2,1,0:T(2,128)(2,1)}), bf16[32,2,2048]{2,1,0:T(2,128)(2,1)S(1)}, u32[]{:S(2)}, u32[]{:S(2)}) async-start(bf16[32,2,2048]{2,1,0:T(2,128)(2,1)} %reshape.112), calls=%async_computation.1 | async-start | bytes 524288 | tf_op jit(solution)/shard_map/all_to_all | solution.py:31
  33.2 9.7 %all-to-all-done.1 = bf16[32,2,2048]{2,1,0:T(2,128)(2,1)S(1)} async-done(((bf16[32,2,2048]{2,1,0:T(2,128)(2,1)}), bf16[32,2,2048]{2,1,0:T(2,128)(2,1)S(1)}, u32[]{:S(2)}, u32[]{:S(2)}) %all-to-all-start.1) | async-done | bytes 262176 | tf_op jit(solution)/shard_map/all_to_all | solution.py:31
  43.5 0.7 broadcast_in_dim.46
  44.2 3.9 %all-to-all-start.2 = ((bf16[32,2,1024]{2,1,0:T(2,128)(2,1)}), bf16[32,2,1024]{2,1,0:T(2,128)(2,1)S(1)}, u32[]{:S(2)}, u32[]{:S(2)}) async-start(bf16[32,2,1024]{2,1,0:T(2,128)(2,1)} %broadcast_in_dim.46), calls=%async_computation.2 | async-start | bytes 262144 | tf_op jit(solution)/shard_map/all_to_all | solution.py:31
  48.5 9.0 %all-to-all-done.2 = bf16[32,2,1024]{2,1,0:T(2,128)(2,1)S(1)} async-done(((bf16[32,2,1024]{2,1,0:T(2,128)(2,1)}), bf16[32,2,1024]{2,1,0:T(2,128)(2,1)S(1)}, u32[]{:S(2)}, u32[]{:S(2)}) %all-to-all-start.2) | async-done | bytes 131104 | tf_op jit(solution)/shard_map/all_to_all | solution.py:31
  57.9 5.2 %collective-permute-start.3 = (f32[64,64]{1,0:T(8,128)S(1)}, f32[64,64]{1,0:T(8,128)S(1)}, u32[]{:S(2)}, u32[]{:S(2)}) collective-permute-start(f32[64,64]{1,0:T(8,128)S(1)} %out_part.1.part), channel_id=1, source_target_pairs={{0,1},{1,0},{2,3},{3,2},{4,5},{5,4},{6,7},{7,6},{8,9},{9,8},{10,11... | collective-permute-start | bytes 49160 | tf_op jit(solution)/shard_map/ppermute | solution.py:36
  63.2 0.7 collective-permute-done.3.other
  63.9 0.9 hidden_pieces.1
  64.8 3.9 %all-to-all-start.3 = ((bf16[32,32,128]{2,1,0:T(8,128)(2,1)}), bf16[32,32,128]{2,1,0:T(8,128)(2,1)S(1)}, u32[]{:S(2)}, u32[]{:S(2)}) async-start(bf16[32,32,128]{2,1,0:T(8,128)(2,1)} %hidden_pieces.1), calls=%async_computation.3 | async-start | bytes 524288 | tf_op jit(solution)/shard_map/all_to_all | solution.py:31
  69.2 11.3 %all-to-all-done.3.pieces = bf16[32,32,128]{2,1,0:T(8,128)(2,1)S(1)} async-done(((bf16[32,32,128]{2,1,0:T(8,128)(2,1)}), bf16[32,32,128]{2,1,0:T(8,128)(2,1)S(1)}, u32[]{:S(2)}, u32[]{:S(2)}) %all-to-all-start.3) | async-done | bytes 262176 | tf_op jit(solution)/shard_map/all_to_all | solution.py:31
  81.1 1.5 %collective-permute-start.4 = (bf16[32,2048]{1,0:T(8,128)(2,1)S(1)}, bf16[32,2048]{1,0:T(8,128)(2,1)S(1)}, u32[]{:S(2)}, u32[]{:S(2)}) collective-permute-start(bf16[32,2048]{1,0:T(8,128)(2,1)S(1)} %get-tuple-element.28), channel_id=1, source_target_pairs={{0,2},{2,4},{4,6},{6,0},{1,3},{3,5},{5,7},{7,1},{8,10},{10,12},{12... | collective-permute-start | bytes 393224 | tf_op jit(solution)/shard_map/ppermute | solution.py:36
  82.6 1.7 %collective-permute-start.5 = (bf16[32,2048]{1,0:T(8,128)(2,1)S(1)}, bf16[32,2048]{1,0:T(8,128)(2,1)S(1)}, u32[]{:S(2)}, u32[]{:S(2)}) collective-permute-start(bf16[32,2048]{1,0:T(8,128)(2,1)S(1)} %get-tuple-element.29), channel_id=1, source_target_pairs={{0,4},{2,6},{4,0},{6,2},{1,5},{3,7},{5,1},{7,3},{8,12},{10,14},{12... | collective-permute-start | bytes 393224 | tf_op jit(solution)/shard_map/ppermute | solution.py:36
  84.3 0.8 collective-permute-start.6
  85.1 3.0 %dense_term.1 = (f32[64,2048]{1,0:T(8,128)S(1)}, f32[1,2048]{1,0:T(1,128)S(1)}, bf16[2048,512]{1,0:T(8,128)(2,1)S(1)}, bf16[2048,512]{1,0:T(8,128)(2,1)S(1)}) custom-call(s32[1]{0:T(128)} %bitcast.own_at, bf16[32,32,128]{2,1,0:T(8,128)(2,1)S(1)} %all-to-all-done.3.pieces, f32[1,2048]{1,0:T(1,128)S(1)} %bitcast.37, f32[1,2048]{1,0:T(1,128)S(1)} %bitcast.38, ...), custom_call_target="tpu_custom_call" | custom-call | flops 67108864 | bytes 3670016 | tf_op jit(solution)/shard_map/dense_term/pallas_call | solution.py:447
  88.4 2.4 %expert.1 = (bf16[32,2048]{1,0:T(8,128)(2,1)S(1)}, bf16[32,2048]{1,0:T(8,128)(2,1)S(1)}, bf16[32,2048]{1,0:T(8,128)(2,1)S(1)}, bf16[32,2048]{1,0:T(8,128)(2,1)S(1)}) custom-call(bf16[32,2048]{1,0:T(8,128)(2,1)S(1)} %get-tuple-element.27.own, bf16[32,2048]{1,0:T(8,128)(2,1)S(1)} %collective-permute-done.4.one, ...), custom_call_target="tpu_custom_call" | custom-call | tf_op jit(solution)/shard_map/expert/pallas_call | solution.py:468
  90.9 2.2 %collective-permute-start.7 = (bf16[32,2048]{1,0:T(8,128)(2,1)S(1)}, bf16[32,2048]{1,0:T(8,128)(2,1)S(1)}, u32[]{:S(2)}, u32[]{:S(2)}) collective-permute-start(bf16[32,2048]{1,0:T(8,128)(2,1)S(1)} %get-tuple-element.34), channel_id=1, source_target_pairs={{0,6},{2,0},{4,2},{6,4},{1,7},{3,1},{5,3},{7,5},{8,14},{10,8},{12,... | collective-permute-start | bytes 393224 | tf_op jit(solution)/shard_map/ppermute | solution.py:36
  93.1 1.1 collective-permute-start.8
  94.2 2.2 %collective-permute-done.7.e1 = bf16[32,2048]{1,0:T(8,128)(2,1)S(1)} collective-permute-done((bf16[32,2048]{1,0:T(8,128)(2,1)S(1)}, bf16[32,2048]{1,0:T(8,128)(2,1)S(1)}, u32[]{:S(2)}, u32[]{:S(2)}) %collective-permute-start.7) | collective-permute-done | bytes 131104 | tf_op jit(solution)/shard_map/ppermute | solution.py:36
  96.4 2.1 %collective-permute-done.8.e2 = bf16[32,2048]{1,0:T(8,128)(2,1)S(1)} collective-permute-done((bf16[32,2048]{1,0:T(8,128)(2,1)S(1)}, bf16[32,2048]{1,0:T(8,128)(2,1)S(1)}, u32[]{:S(2)}, u32[]{:S(2)}) %collective-permute-start.8) | collective-permute-done | bytes 131104 | tf_op jit(solution)/shard_map/ppermute | solution.py:36
  98.4 1.3 %collective-permute-done.9.e3 = bf16[32,2048]{1,0:T(8,128)(2,1)S(1)} collective-permute-done((bf16[32,2048]{1,0:T(8,128)(2,1)S(1)}, bf16[32,2048]{1,0:T(8,128)(2,1)S(1)}, u32[]{:S(2)}, u32[]{:S(2)}) %collective-permute-start.9) | collective-permute-done | bytes 131104 | tf_op jit(solution)/shard_map/ppermute | solution.py:36
  100.0 0.9 reshape.114
  100.9 9.3 %all-to-all-start.4 = ((bf16[32,2,2048]{2,1,0:T(2,128)(2,1)}), bf16[32,2,2048]{2,1,0:T(2,128)(2,1)S(1)}, u32[]{:S(2)}, u32[]{:S(2)}) async-start(bf16[32,2,2048]{2,1,0:T(2,128)(2,1)} %reshape.114), calls=%async_computation.4 | async-start | bytes 524288 | tf_op jit(solution)/shard_map/all_to_all | solution.py:31
  111.0 2.6 %multiply_add_fusion = f32[2,16,64,128]{3,2,1,0:T(8,128)} fusion(f32[2,16,64,128]{3,2,1,0:T(8,128)} %param.27, f32[2,16,128]{2,1,0:T(8,128)S(1)} %broadcast_bitcast_fusion, f32[2,16,64]{2,1,0:T(8,128)S(1)} %multiply_multiply_fusion, f32[2,16]{1,0:T(2,128)S(1)} %get-tuple-element.47), kind=kLoop, calls=%fused_computation.5 | loop fusion | flops 786432 | bytes 2121856 | tf_op jit(solution)/shard_map/add | solution.py:288
  113.6 7.7 %all-to-all-done.4 = bf16[32,2,2048]{2,1,0:T(2,128)(2,1)S(1)} async-done(((bf16[32,2,2048]{2,1,0:T(2,128)(2,1)}), bf16[32,2,2048]{2,1,0:T(2,128)(2,1)S(1)}, u32[]{:S(2)}, u32[]{:S(2)}) %all-to-all-start.4) | async-done | bytes 262176 | tf_op jit(solution)/shard_map/all_to_all | solution.py:31
  121.5 2.7 %collective-permute-start.10 = (f32[1,2048]{1,0:T(1,128)S(1)}, f32[1,2048]{1,0:T(1,128)S(1)}, u32[]{:S(2)}, u32[]{:S(2)}) collective-permute-start(f32[1,2048]{1,0:T(1,128)S(1)} %broadcast_select_fusion), channel_id=1, source_target_pairs={{0,1},{1,0},{2,3},{3,2},{4,5},{5,4},{6,7},{7,6},{8,9},{9,8},{10,11... | collective-permute-start | bytes 24584 | tf_op jit(solution)/shard_map/ppermute | solution.py:36
  124.2 0.6 fusion.6
  (98 shorter events, 8.1 us)
Async XLA Ops:
  0.6 17.6 %copy-start = (bf16[2048,256]{1,0:T(8,128)(2,1)S(1)}, bf16[2048,256]{1,0:T(8,128)(2,1)}, u32[]{:S(2)}) copy-start(bf16[2048,256]{1,0:T(8,128)(2,1)} %param.33) | copy-start | bytes 3145732
  0.7 19.3 %copy-start.7 = (bf16[2,3,2,256]{3,2,1,0:T(2,128)(2,1)S(1)}, bf16[2,3,2,256]{3,2,1,0:T(2,128)(2,1)}, u32[]{:S(2)}) copy-start(bf16[2,3,2,256]{3,2,1,0:T(2,128)(2,1)} %param.29) | copy-start | bytes 18436
  0.7 19.4 %copy-start.6 = (f32[4,2,256]{2,1,0:T(2,128)S(1)}, f32[4,2,256]{2,1,0:T(2,128)}, u32[]{:S(2)}) copy-start(f32[4,2,256]{2,1,0:T(2,128)} %param.37) | copy-start | bytes 24580
  0.7 19.7 %copy-start.10 = (f32[16]{0:T(128)S(1)}, f32[16]{0:T(128)}, u32[]{:S(2)}) copy-start(f32[16]{0:T(128)} %param.39) | copy-start | bytes 196
  0.7 19.7 %copy-start.9 = (bf16[2048,16]{0,1:T(8,128)(2,1)S(1)}, bf16[2048,16]{0,1:T(8,128)(2,1)}, u32[]{:S(2)}) copy-start(bf16[2048,16]{0,1:T(8,128)(2,1)} %param.35) | copy-start | bytes 196612
  0.7 19.7 %copy-start.12 = (f32[16]{0:T(128)S(1)}, f32[16]{0:T(128)}, u32[]{:S(2)}) copy-start(f32[16]{0:T(128)} %param.38) | copy-start | bytes 196
  0.7 19.7 %copy-start.11 = (f32[16]{0:T(128)S(1)}, f32[16]{0:T(128)}, u32[]{:S(2)}) copy-start(f32[16]{0:T(128)} %param.40) | copy-start | bytes 196
  0.7 19.9 %copy-start.3 = (f32[2,16,64,128]{3,2,1,0:T(8,128)S(1)}, f32[2,16,64,128]{3,2,1,0:T(8,128)}, u32[]{:S(2)}) copy-start(f32[2,16,64,128]{3,2,1,0:T(8,128)} %param.27) | copy-start | bytes 3145732
  2.6 24.4 %collective-permute-start = (bf16[56,2048]{1,0:T(8,128)(2,1)S(1)}, bf16[56,2048]{1,0:T(8,128)(2,1)S(1)}, u32[]{:S(2)}, u32[]{:S(2)}) collective-permute-start(bf16[56,2048]{1,0:T(8,128)(2,1)S(1)} %get-tuple-element.23.h0), channel_id=1, source_target_pairs={{0,6},{2,0},{4,2},{6,4},{1,7},{3,1},{5,3},{7,5},{8,14},{10,8},{12,... | collective-permute-start | bytes 688136 | tf_op jit(solution)/shard_map/ppermute | solution.py:36
  5.9 21.1 %collective-permute-start.1 = (bf16[56,2048]{1,0:T(8,128)(2,1)S(1)}, bf16[56,2048]{1,0:T(8,128)(2,1)S(1)}, u32[]{:S(2)}, u32[]{:S(2)}) collective-permute-start(bf16[56,2048]{1,0:T(8,128)(2,1)S(1)} %get-tuple-element.23.h0), channel_id=1, source_target_pairs={{0,4},{2,6},{4,0},{6,2},{1,5},{3,7},{5,1},{7,3},{8,12},{10,14},{12... | collective-permute-start | bytes 688136 | tf_op jit(solution)/shard_map/ppermute | solution.py:36
  6.4 20.6 %collective-permute-start.2 = (bf16[56,2048]{1,0:T(8,128)(2,1)S(1)}, bf16[56,2048]{1,0:T(8,128)(2,1)S(1)}, u32[]{:S(2)}, u32[]{:S(2)}) collective-permute-start(bf16[56,2048]{1,0:T(8,128)(2,1)S(1)} %get-tuple-element.23.h0), channel_id=1, source_target_pairs={{0,2},{2,4},{4,6},{6,0},{1,3},{3,5},{5,7},{7,1},{8,10},{10,12},{12... | collective-permute-start | bytes 688136 | tf_op jit(solution)/shard_map/ppermute | solution.py:36
  7.0 19.9 %all-to-all-start = ((bf16[32,2,256]{2,1,0:T(2,128)(2,1)}), bf16[32,2,256]{2,1,0:T(2,128)(2,1)S(1)}, u32[]{:S(2)}, u32[]{:S(2)}) async-start(bf16[32,2,256]{2,1,0:T(2,128)(2,1)} %get-tuple-element.22), calls=%async_computation | async-start | bytes 65536 | tf_op jit(solution)/shard_map/all_to_all | solution.py:31
  20.0 23.2 %copy-start.4 = (bf16[2,3,1024]{2,0,1:T(2,128)(2,1)S(1)}, bf16[2,3,1024]{2,0,1:T(2,128)(2,1)}, u32[]{:S(2)}) copy-start(bf16[2,3,1024]{2,0,1:T(2,128)(2,1)} %param.28) | copy-start | bytes 36868
  20.0 23.2 %copy-start.5 = (f32[4,1024]{1,0:T(4,128)S(1)}, f32[4,1024]{1,0:T(4,128)}, u32[]{:S(2)}) copy-start(f32[4,1024]{1,0:T(4,128)} %param.36) | copy-start | bytes 49156
  20.1 23.4 %copy-start.8 = (f32[1024]{0:T(1024)S(1)}, f32[1024]{0:T(1024)}, u32[]{:S(2)}) copy-start(f32[1024]{0:T(1024)} %param.41) | copy-start | bytes 12292
  28.2 52.3 %copy-start.1 = (f32[2048]{0:T(1024)S(1)}, f32[2048]{0:T(1024)}, u32[]{:S(2)}) copy-start(f32[2048]{0:T(1024)} %param.43) | copy-start | bytes 24580
  28.2 14.7 %all-to-all-start.1 = ((bf16[32,2,2048]{2,1,0:T(2,128)(2,1)}), bf16[32,2,2048]{2,1,0:T(2,128)(2,1)S(1)}, u32[]{:S(2)}, u32[]{:S(2)}) async-start(bf16[32,2,2048]{2,1,0:T(2,128)(2,1)} %reshape.112), calls=%async_computation.1 | async-start | bytes 524288 | tf_op jit(solution)/shard_map/all_to_all | solution.py:31
  32.4 52.7 %copy-start.2 = (f32[2048]{0:T(1024)S(1)}, f32[2048]{0:T(1024)}, u32[]{:S(2)}) copy-start(f32[2048]{0:T(1024)} %param.51) | copy-start | bytes 24580
  44.2 13.3 %all-to-all-start.2 = ((bf16[32,2,1024]{2,1,0:T(2,128)(2,1)}), bf16[32,2,1024]{2,1,0:T(2,128)(2,1)S(1)}, u32[]{:S(2)}, u32[]{:S(2)}) async-start(bf16[32,2,1024]{2,1,0:T(2,128)(2,1)} %broadcast_in_dim.46), calls=%async_computation.2 | async-start | bytes 262144 | tf_op jit(solution)/shard_map/all_to_all | solution.py:31
  57.9 6.0 %collective-permute-start.3 = (f32[64,64]{1,0:T(8,128)S(1)}, f32[64,64]{1,0:T(8,128)S(1)}, u32[]{:S(2)}, u32[]{:S(2)}) collective-permute-start(f32[64,64]{1,0:T(8,128)S(1)} %out_part.1.part), channel_id=1, source_target_pairs={{0,1},{1,0},{2,3},{3,2},{4,5},{5,4},{6,7},{7,6},{8,9},{9,8},{10,11... | collective-permute-start | bytes 49160 | tf_op jit(solution)/shard_map/ppermute | solution.py:36
  64.8 15.7 %all-to-all-start.3 = ((bf16[32,32,128]{2,1,0:T(8,128)(2,1)}), bf16[32,32,128]{2,1,0:T(8,128)(2,1)S(1)}, u32[]{:S(2)}, u32[]{:S(2)}) async-start(bf16[32,32,128]{2,1,0:T(8,128)(2,1)} %hidden_pieces.1), calls=%async_computation.3 | async-start | bytes 524288 | tf_op jit(solution)/shard_map/all_to_all | solution.py:31
  81.1 7.1 %collective-permute-start.4 = (bf16[32,2048]{1,0:T(8,128)(2,1)S(1)}, bf16[32,2048]{1,0:T(8,128)(2,1)S(1)}, u32[]{:S(2)}, u32[]{:S(2)}) collective-permute-start(bf16[32,2048]{1,0:T(8,128)(2,1)S(1)} %get-tuple-element.28), channel_id=1, source_target_pairs={{0,2},{2,4},{4,6},{6,0},{1,3},{3,5},{5,7},{7,1},{8,10},{10,12},{12... | collective-permute-start | bytes 393224 | tf_op jit(solution)/shard_map/ppermute | solution.py:36
  82.6 5.8 %collective-permute-start.5 = (bf16[32,2048]{1,0:T(8,128)(2,1)S(1)}, bf16[32,2048]{1,0:T(8,128)(2,1)S(1)}, u32[]{:S(2)}, u32[]{:S(2)}) collective-permute-start(bf16[32,2048]{1,0:T(8,128)(2,1)S(1)} %get-tuple-element.29), channel_id=1, source_target_pairs={{0,4},{2,6},{4,0},{6,2},{1,5},{3,7},{5,1},{7,3},{8,12},{10,14},{12... | collective-permute-start | bytes 393224 | tf_op jit(solution)/shard_map/ppermute | solution.py:36
  84.3 4.1 %collective-permute-start.6 = (bf16[32,2048]{1,0:T(8,128)(2,1)S(1)}, bf16[32,2048]{1,0:T(8,128)(2,1)S(1)}, u32[]{:S(2)}, u32[]{:S(2)}) collective-permute-start(bf16[32,2048]{1,0:T(8,128)(2,1)S(1)} %get-tuple-element.30), channel_id=1, source_target_pairs={{0,6},{2,0},{4,2},{6,4},{1,7},{3,1},{5,3},{7,5},{8,14},{10,8},{12,... | collective-permute-start | bytes 393224 | tf_op jit(solution)/shard_map/ppermute | solution.py:36
  90.9 5.5 %collective-permute-start.7 = (bf16[32,2048]{1,0:T(8,128)(2,1)S(1)}, bf16[32,2048]{1,0:T(8,128)(2,1)S(1)}, u32[]{:S(2)}, u32[]{:S(2)}) collective-permute-start(bf16[32,2048]{1,0:T(8,128)(2,1)S(1)} %get-tuple-element.34), channel_id=1, source_target_pairs={{0,6},{2,0},{4,2},{6,4},{1,7},{3,1},{5,3},{7,5},{8,14},{10,8},{12,... | collective-permute-start | bytes 393224 | tf_op jit(solution)/shard_map/ppermute | solution.py:36
  93.1 5.4 %collective-permute-start.8 = (bf16[32,2048]{1,0:T(8,128)(2,1)S(1)}, bf16[32,2048]{1,0:T(8,128)(2,1)S(1)}, u32[]{:S(2)}, u32[]{:S(2)}) collective-permute-start(bf16[32,2048]{1,0:T(8,128)(2,1)S(1)} %get-tuple-element.35), channel_id=1, source_target_pairs={{0,4},{2,6},{4,0},{6,2},{1,5},{3,7},{5,1},{7,3},{8,12},{10,14},{12... | collective-permute-start | bytes 393224 | tf_op jit(solution)/shard_map/ppermute | solution.py:36
  94.2 5.6 %collective-permute-start.9 = (bf16[32,2048]{1,0:T(8,128)(2,1)S(1)}, bf16[32,2048]{1,0:T(8,128)(2,1)S(1)}, u32[]{:S(2)}, u32[]{:S(2)}) collective-permute-start(bf16[32,2048]{1,0:T(8,128)(2,1)S(1)} %get-tuple-element.36), channel_id=1, source_target_pairs={{0,2},{2,4},{4,6},{6,0},{1,3},{3,5},{5,7},{7,1},{8,10},{10,12},{12... | collective-permute-start | bytes 393224 | tf_op jit(solution)/shard_map/ppermute | solution.py:36
  100.9 20.4 %all-to-all-start.4 = ((bf16[32,2,2048]{2,1,0:T(2,128)(2,1)}), bf16[32,2,2048]{2,1,0:T(2,128)(2,1)S(1)}, u32[]{:S(2)}, u32[]{:S(2)}) async-start(bf16[32,2,2048]{2,1,0:T(2,128)(2,1)} %reshape.114), calls=%async_computation.4 | async-start | bytes 524288 | tf_op jit(solution)/shard_map/all_to_all | solution.py:31
  121.5 3.5 %collective-permute-start.10 = (f32[1,2048]{1,0:T(1,128)S(1)}, f32[1,2048]{1,0:T(1,128)S(1)}, u32[]{:S(2)}, u32[]{:S(2)}) collective-permute-start(f32[1,2048]{1,0:T(1,128)S(1)} %broadcast_select_fusion), channel_id=1, source_target_pairs={{0,1},{1,0},{2,3},{3,2},{4,5},{5,4},{6,7},{7,6},{8,9},{9,8},{10,11... | collective-permute-start | bytes 24584 | tf_op jit(solution)/shard_map/ppermute | solution.py:36

commit v4 on v3

--- a/solution.py
+++ b/solution.py
@@ -102,7 +102,8 @@
     turn = (row == (column + share * line_at[0]) % block).astype(bf16)
     turned = jnp.dot(spread[:, :block], turn, preferred_element_type=f32).astype(bf16)
     weight = jnp.concatenate([h[:share, :] for h in (h0, h1, h2, h3)], axis=0)
-    part[...] = jnp.dot(turned, weight, preferred_element_type=f32).astype(bf16)
+    result = jnp.dot(turned, weight, preferred_element_type=f32).astype(bf16)
+    part[...] = result.reshape(part.shape)
 
 
 def out_kernel(line_at, mixer, h0, h1, h2, h3, part):
@@ -212,7 +213,7 @@
 def combine_kernel(placed, dense_term, e0, e1, e2, e3, terms):
     rows = jnp.concatenate([e0[...], e1[...], e2[...], e3[...]], axis=0)
     mix = jnp.dot(placed[...], rows, preferred_element_type=f32)
-    terms[...] = (mix + dense_term[...]).astype(bf16)
+    terms[...] = (mix + dense_term[...]).astype(bf16).reshape(terms.shape)
 
 
 def expert_kernel(own, one, two, three, gate, up, down, r0, r1, r2, r3, down_near, sems):
@@ -361,19 +362,17 @@
     )
     spread = exchanged(features, ROW_AXES)
     spread = spread.reshape(batch, lanes)
-    all_routes = spread[:, 2 * block : 2 * block + topk]
-    all_logits = spread[:, 2 * block + topk : 2 * block + 2 * topk].astype(f32)
 
     lines = [held] + [shifted(held, "x", -by) for by in range(1, line_n)]
     in_part = pl.pallas_call(
         in_kernel,
-        out_shape=pltpu.VMEM((batch, width), bf16),
+        out_shape=jax.ShapeDtypeStruct((rows_n, seq_count, width), bf16),
         in_specs=[smem] + [vmem] * (1 + line_n),
         out_specs=vmem,
         name="in_part",
         compiler_params=pltpu.CompilerParams(vmem_limit_bytes=8 << 20),
     )(line_at.reshape(1), *in_vmem(spread, *lines))
-    in_terms = exchanged(in_part.reshape(rows_n, seq_count, 2 * channels), ROW_AXES)
+    in_terms = exchanged(in_part, ROW_AXES)
     in_sum = jnp.sum(in_terms.astype(f32), axis=0).astype(bf16)
     gate_proj, inner_proj = in_sum[:, :channels], in_sum[:, channels:]
     write_proj = jnp.dot(normed_in, write_weight, preferred_element_type=f32).astype(bf16)
@@ -418,6 +417,8 @@
     )(*in_vmem(mixed_part, other_part, spread))
     hidden = exchanged(pieces, ROW_AXES)
 
+    all_routes = spread[:, 2 * block : 2 * block + topk]
+    all_logits = spread[:, 2 * block + topk : 2 * block + 2 * topk].astype(f32)
     route_gates = jax.nn.softmax(all_logits, axis=-1)
     experts = (line_n * row_at + (line_at + jnp.arange(line_n)) % line_n).astype(bf16)
     hits = all_routes[None] == experts[:, None, None]
@@ -480,13 +481,13 @@
     returned = [expert_rows[0]] + [shifted(expert_rows[by], "x", -by) for by in range(1, line_n)]
     terms = pl.pallas_call(
         combine_kernel,
-        out_shape=pltpu.VMEM((batch, width), bf16),
+        out_shape=jax.ShapeDtypeStruct((rows_n, seq_count, width), bf16),
         in_specs=[vmem] * (2 + line_n),
         out_specs=vmem,
         name="terms",
         compiler_params=pltpu.CompilerParams(vmem_limit_bytes=8 << 20),
     )(*in_vmem(placed, dense_term, *returned))
-    terms = exchanged(terms.reshape(rows_n, seq_count, width), ROW_AXES)
+    terms = exchanged(terms, ROW_AXES)
     sums = jnp.sum(terms.astype(f32), axis=0)
     other = jnp.where(tp_at == 0, sums[1:], sums[:1])
     mine = jnp.where(tp_at == 0, sums[:1], sums[1:])

time: 126 us -> 126 us (level)
  local copies, waits for them, and re-layouts: 4.51 us -> 2.72 us
  Pallas kernels: 9.66 us -> 11.1 us
    reshape x2 -> x0, local copies, waits for them, and re-layouts: 1.79 us -> none  [the longest x1 0.9 us: local(): terms = exchanged(terms.reshape(rows_n, seq_count, width), ROW_AXES)]
    pallas_call x2, Pallas kernels: 0.56 us -> 1.99 us  [the longest x1 1.05 us: local(): pl.pallas_call(in_kernel, out_shape=jax.ShapeDtypeStruct((rows_n, seq_cou...]
  transfers between devices with their start and end apart: 16 -> 16, of which waited for: 12 -> 12; matrix products, arithmetic and copies ran while one was open for 7% -> 6% of each run, Pallas kernels for 2% -> 2%
where the time goes in v4:
time: 126 us; the launch traced here: 125 us
  starting transfers between devices  52.1 us (41%)
  waiting for transfers between devices  51.7 us (41%)
  Pallas kernels  11.1 us (9%)
  other arithmetic  4.58 us (4%)
  local copies, waits for them, and re-layouts  2.72 us (2%)
  matrix products  2.01 us (2%)
    all_to_all x5, waiting for transfers between devices, exchanged(): return lax.all_to_all(pieces, axis, split_axis=0, concat_axis=0, tiled=True)  44.9 us
    all_to_all x5, starting transfers between devices, exchanged(): return lax.all_to_all(pieces, axis, split_axis=0, concat_axis=0, tiled=True)  32.4 us
    ppermute x11, starting transfers between devices, shifted(): lax.ppermute(block, axis, [(i, (i + by) % size) for i in range(size)])  19.6 us
    ppermute x11, waiting for transfers between devices, shifted(): lax.ppermute(block, axis, [(i, (i + by) % size) for i in range(size)])  6.78 us
    pallas_call x1, Pallas kernels, local(): pl.pallas_call(dense_kernel, out_shape=(pltpu.VMEM((batch, width), f32),...  3.03 us
  transfers between devices with their start and end apart: 16, of which 12 were waited for; matrix products, arithmetic and copies ran while one was open for 6% of the time, Pallas kernels for 2%

profile of v4, /device:TPU:1, one launch (start us, length us, event | category | flops | bytes accessed | tf_op | source)
XLA Modules:
  0.0 125.3 jit_solution(5744825606619333773)
XLA Ops:
  0.7 1.9 %start.1 = (bf16[32,2,256]{2,1,0:T(2,128)(2,1)}, bf16[2,2048]{1,0:T(2,128)(2,1)S(1)}, bf16[56,2048]{1,0:T(8,128)(2,1)S(1)}) custom-call(bf16[2,2048]{1,0:T(2,128)(2,1)} %tokens.1, f32[1,2048]{1,0:T(1,128)} %bitcast.49, s32[2,4]{1,0:T(2,128)} %routes.1, bf16[2,4]{1,0:T(2,128)(2,1)} %logits.1, bf16[16,1024]{1,0:T(8,128)(2,1)} %gate_weight.1, ...), custom_call_target="tpu_custom_call" | custom-call | tf_op jit(solution)/shard_map/start/pallas_call | solution.py:340
  2.6 3.3 %collective-permute-start = (bf16[56,2048]{1,0:T(8,128)(2,1)S(1)}, bf16[56,2048]{1,0:T(8,128)(2,1)S(1)}, u32[]{:S(2)}, u32[]{:S(2)}) collective-permute-start(bf16[56,2048]{1,0:T(8,128)(2,1)S(1)} %get-tuple-element.23.h0), channel_id=1, source_target_pairs={{0,6},{2,0},{4,2},{6,4},{1,7},{3,1},{5,3},{7,5},{8,14},{10,8},{12,... | collective-permute-start | bytes 688136 | tf_op jit(solution)/shard_map/ppermute | solution.py:36
  7.0 11.2 %all-to-all-start = ((bf16[32,2,256]{2,1,0:T(2,128)(2,1)}), bf16[32,2,256]{2,1,0:T(2,128)(2,1)S(1)}, u32[]{:S(2)}, u32[]{:S(2)}) async-start(bf16[32,2,256]{2,1,0:T(2,128)(2,1)} %get-tuple-element.22), calls=%async_computation | async-start | bytes 65536 | tf_op jit(solution)/shard_map/all_to_all | solution.py:31
  18.5 1.5 %fusion.1 = bf16[2,1,256]{2,0,1:T(2,128)(2,1)S(1)} fusion(bf16[2,2048]{1,0:T(2,128)(2,1)S(1)} %get-tuple-element.21, bf16[2048,256]{1,0:T(8,128)(2,1)} %param.34), kind=kOutput, calls=%fused_computation.3 | convolution fusion | flops 2097664 | bytes 1057792 | tf_op jit(solution)/shard_map/dot_general | solution.py:379
  20.9 6.0 %all-to-all-done = bf16[32,2,256]{2,1,0:T(2,128)(2,1)S(1)} async-done(((bf16[32,2,256]{2,1,0:T(2,128)(2,1)}), bf16[32,2,256]{2,1,0:T(2,128)(2,1)S(1)}, u32[]{:S(2)}, u32[]{:S(2)}) %all-to-all-start) | async-done | bytes 32800 | tf_op jit(solution)/shard_map/all_to_all | solution.py:31
  27.0 1.1 in_part.1
  28.1 4.2 %all-to-all-start.1 = ((bf16[32,2,2048]{2,1,0:T(2,128)(2,1)}), bf16[32,2,2048]{2,1,0:T(2,128)(2,1)S(1)}, u32[]{:S(2)}, u32[]{:S(2)}) async-start(bf16[32,2,2048]{2,1,0:T(2,128)(2,1)} %in_part.1), calls=%async_computation.1 | async-start | bytes 524288 | tf_op jit(solution)/shard_map/all_to_all | solution.py:31
  33.1 9.7 %all-to-all-done.1 = bf16[32,2,2048]{2,1,0:T(2,128)(2,1)S(1)} async-done(((bf16[32,2,2048]{2,1,0:T(2,128)(2,1)}), bf16[32,2,2048]{2,1,0:T(2,128)(2,1)S(1)}, u32[]{:S(2)}, u32[]{:S(2)}) %all-to-all-start.1) | async-done | bytes 262176 | tf_op jit(solution)/shard_map/all_to_all | solution.py:31
  43.3 0.7 broadcast_in_dim.46
  44.0 3.9 %all-to-all-start.2 = ((bf16[32,2,1024]{2,1,0:T(2,128)(2,1)}), bf16[32,2,1024]{2,1,0:T(2,128)(2,1)S(1)}, u32[]{:S(2)}, u32[]{:S(2)}) async-start(bf16[32,2,1024]{2,1,0:T(2,128)(2,1)} %broadcast_in_dim.46), calls=%async_computation.2 | async-start | bytes 262144 | tf_op jit(solution)/shard_map/all_to_all | solution.py:31
  48.3 9.0 %all-to-all-done.2 = bf16[32,2,1024]{2,1,0:T(2,128)(2,1)S(1)} async-done(((bf16[32,2,1024]{2,1,0:T(2,128)(2,1)}), bf16[32,2,1024]{2,1,0:T(2,128)(2,1)S(1)}, u32[]{:S(2)}, u32[]{:S(2)}) %all-to-all-start.2) | async-done | bytes 131104 | tf_op jit(solution)/shard_map/all_to_all | solution.py:31
  57.7 5.2 %collective-permute-start.3 = (f32[64,64]{1,0:T(8,128)S(1)}, f32[64,64]{1,0:T(8,128)S(1)}, u32[]{:S(2)}, u32[]{:S(2)}) collective-permute-start(f32[64,64]{1,0:T(8,128)S(1)} %out_part.1.part), channel_id=1, source_target_pairs={{0,1},{1,0},{2,3},{3,2},{4,5},{5,4},{6,7},{7,6},{8,9},{9,8},{10,11... | collective-permute-start | bytes 49160 | tf_op jit(solution)/shard_map/ppermute | solution.py:36
  63.0 0.7 collective-permute-done.3.other
  63.7 0.9 hidden_pieces.1
  64.6 3.9 %all-to-all-start.3 = ((bf16[32,32,128]{2,1,0:T(8,128)(2,1)}), bf16[32,32,128]{2,1,0:T(8,128)(2,1)S(1)}, u32[]{:S(2)}, u32[]{:S(2)}) async-start(bf16[32,32,128]{2,1,0:T(8,128)(2,1)} %hidden_pieces.1), calls=%async_computation.3 | async-start | bytes 524288 | tf_op jit(solution)/shard_map/all_to_all | solution.py:31
  69.0 11.3 %all-to-all-done.3.pieces = bf16[32,32,128]{2,1,0:T(8,128)(2,1)S(1)} async-done(((bf16[32,32,128]{2,1,0:T(8,128)(2,1)}), bf16[32,32,128]{2,1,0:T(8,128)(2,1)S(1)}, u32[]{:S(2)}, u32[]{:S(2)}) %all-to-all-start.3) | async-done | bytes 262176 | tf_op jit(solution)/shard_map/all_to_all | solution.py:31
  80.9 1.5 %collective-permute-start.4 = (bf16[32,2048]{1,0:T(8,128)(2,1)S(1)}, bf16[32,2048]{1,0:T(8,128)(2,1)S(1)}, u32[]{:S(2)}, u32[]{:S(2)}) collective-permute-start(bf16[32,2048]{1,0:T(8,128)(2,1)S(1)} %get-tuple-element.28), channel_id=1, source_target_pairs={{0,2},{2,4},{4,6},{6,0},{1,3},{3,5},{5,7},{7,1},{8,10},{10,12},{12... | collective-permute-start | bytes 393224 | tf_op jit(solution)/shard_map/ppermute | solution.py:36
  82.4 1.7 %collective-permute-start.5 = (bf16[32,2048]{1,0:T(8,128)(2,1)S(1)}, bf16[32,2048]{1,0:T(8,128)(2,1)S(1)}, u32[]{:S(2)}, u32[]{:S(2)}) collective-permute-start(bf16[32,2048]{1,0:T(8,128)(2,1)S(1)} %get-tuple-element.29), channel_id=1, source_target_pairs={{0,4},{2,6},{4,0},{6,2},{1,5},{3,7},{5,1},{7,3},{8,12},{10,14},{12... | collective-permute-start | bytes 393224 | tf_op jit(solution)/shard_map/ppermute | solution.py:36
  84.1 0.8 collective-permute-start.6
  84.9 3.0 %dense_term.1 = (f32[64,2048]{1,0:T(8,128)S(1)}, f32[1,2048]{1,0:T(1,128)S(1)}, bf16[2048,512]{1,0:T(8,128)(2,1)S(1)}, bf16[2048,512]{1,0:T(8,128)(2,1)S(1)}) custom-call(s32[1]{0:T(128)} %bitcast.own_at, bf16[32,32,128]{2,1,0:T(8,128)(2,1)S(1)} %all-to-all-done.3.pieces, f32[1,2048]{1,0:T(1,128)S(1)} %bitcast.37, f32[1,2048]{1,0:T(1,128)S(1)} %bitcast.38, ...), custom_call_target="tpu_custom_call" | custom-call | flops 67108864 | bytes 3670016 | tf_op jit(solution)/shard_map/dense_term/pallas_call | solution.py:448
  88.3 2.4 %expert.1 = (bf16[32,2048]{1,0:T(8,128)(2,1)S(1)}, bf16[32,2048]{1,0:T(8,128)(2,1)S(1)}, bf16[32,2048]{1,0:T(8,128)(2,1)S(1)}, bf16[32,2048]{1,0:T(8,128)(2,1)S(1)}) custom-call(bf16[32,2048]{1,0:T(8,128)(2,1)S(1)} %get-tuple-element.27.own, bf16[32,2048]{1,0:T(8,128)(2,1)S(1)} %collective-permute-done.4.one, ...), custom_call_target="tpu_custom_call" | custom-call | tf_op jit(solution)/shard_map/expert/pallas_call | solution.py:469
  90.7 2.1 %collective-permute-start.7 = (bf16[32,2048]{1,0:T(8,128)(2,1)S(1)}, bf16[32,2048]{1,0:T(8,128)(2,1)S(1)}, u32[]{:S(2)}, u32[]{:S(2)}) collective-permute-start(bf16[32,2048]{1,0:T(8,128)(2,1)S(1)} %get-tuple-element.34), channel_id=1, source_target_pairs={{0,6},{2,0},{4,2},{6,4},{1,7},{3,1},{5,3},{7,5},{8,14},{10,8},{12,... | collective-permute-start | bytes 393224 | tf_op jit(solution)/shard_map/ppermute | solution.py:36
  92.9 1.1 collective-permute-start.8
  94.0 2.2 %collective-permute-done.7.e1 = bf16[32,2048]{1,0:T(8,128)(2,1)S(1)} collective-permute-done((bf16[32,2048]{1,0:T(8,128)(2,1)S(1)}, bf16[32,2048]{1,0:T(8,128)(2,1)S(1)}, u32[]{:S(2)}, u32[]{:S(2)}) %collective-permute-start.7) | collective-permute-done | bytes 131104 | tf_op jit(solution)/shard_map/ppermute | solution.py:36
  96.2 2.1 %collective-permute-done.8.e2 = bf16[32,2048]{1,0:T(8,128)(2,1)S(1)} collective-permute-done((bf16[32,2048]{1,0:T(8,128)(2,1)S(1)}, bf16[32,2048]{1,0:T(8,128)(2,1)S(1)}, u32[]{:S(2)}, u32[]{:S(2)}) %collective-permute-start.8) | collective-permute-done | bytes 131104 | tf_op jit(solution)/shard_map/ppermute | solution.py:36
  98.3 1.3 %collective-permute-done.9.e3 = bf16[32,2048]{1,0:T(8,128)(2,1)S(1)} collective-permute-done((bf16[32,2048]{1,0:T(8,128)(2,1)S(1)}, bf16[32,2048]{1,0:T(8,128)(2,1)S(1)}, u32[]{:S(2)}, u32[]{:S(2)}) %collective-permute-start.9) | collective-permute-done | bytes 131104 | tf_op jit(solution)/shard_map/ppermute | solution.py:36
  99.6 0.9 terms.1
  100.5 9.3 %all-to-all-start.4 = ((bf16[32,2,2048]{2,1,0:T(2,128)(2,1)}), bf16[32,2,2048]{2,1,0:T(2,128)(2,1)S(1)}, u32[]{:S(2)}, u32[]{:S(2)}) async-start(bf16[32,2,2048]{2,1,0:T(2,128)(2,1)} %terms.1), calls=%async_computation.4 | async-start | bytes 524288 | tf_op jit(solution)/shard_map/all_to_all | solution.py:31
  110.6 1.4 %multiply_add_fusion = f32[2,16,64,128]{3,2,1,0:T(8,128)} fusion(f32[2,16,64,128]{3,2,1,0:T(8,128)S(1)} %copy-done.4, f32[2,16,128]{2,1,0:T(8,128)S(1)} %broadcast_bitcast_fusion, f32[2,16,64]{2,1,0:T(8,128)S(1)} %multiply_multiply_fusion, f32[2,16]{1,0:T(2,128)S(1)} %get-tuple-element.47), kind=kLoop, calls=%fused_computation.5 | loop fusion | flops 786432 | bytes 2121856 | tf_op jit(solution)/shard_map/add | solution.py:289
  112.0 8.8 %all-to-all-done.4 = bf16[32,2,2048]{2,1,0:T(2,128)(2,1)S(1)} async-done(((bf16[32,2,2048]{2,1,0:T(2,128)(2,1)}), bf16[32,2,2048]{2,1,0:T(2,128)(2,1)S(1)}, u32[]{:S(2)}, u32[]{:S(2)}) %all-to-all-start.4) | async-done | bytes 262176 | tf_op jit(solution)/shard_map/all_to_all | solution.py:31
  121.1 2.7 %collective-permute-start.10 = (f32[1,2048]{1,0:T(1,128)S(1)}, f32[1,2048]{1,0:T(1,128)S(1)}, u32[]{:S(2)}, u32[]{:S(2)}) collective-permute-start(f32[1,2048]{1,0:T(1,128)S(1)} %broadcast_select_fusion), channel_id=1, source_target_pairs={{0,1},{1,0},{2,3},{3,2},{4,5},{5,4},{6,7},{7,6},{8,9},{9,8},{10,11... | collective-permute-start | bytes 24584 | tf_op jit(solution)/shard_map/ppermute | solution.py:36
  123.8 0.6 fusion.6
  (98 shorter events, 7.6 us)
Async XLA Ops:
  0.6 17.6 %copy-start = (bf16[2048,256]{1,0:T(8,128)(2,1)S(1)}, bf16[2048,256]{1,0:T(8,128)(2,1)}, u32[]{:S(2)}) copy-start(bf16[2048,256]{1,0:T(8,128)(2,1)} %param.33) | copy-start | bytes 3145732
  0.7 19.4 %copy-start.8 = (bf16[2,3,2,256]{3,2,1,0:T(2,128)(2,1)S(1)}, bf16[2,3,2,256]{3,2,1,0:T(2,128)(2,1)}, u32[]{:S(2)}) copy-start(bf16[2,3,2,256]{3,2,1,0:T(2,128)(2,1)} %param.29) | copy-start | bytes 18436
  0.7 19.4 %copy-start.7 = (f32[4,2,256]{2,1,0:T(2,128)S(1)}, f32[4,2,256]{2,1,0:T(2,128)}, u32[]{:S(2)}) copy-start(f32[4,2,256]{2,1,0:T(2,128)} %param.37) | copy-start | bytes 24580
  0.7 19.7 %copy-start.11 = (f32[16]{0:T(128)S(1)}, f32[16]{0:T(128)}, u32[]{:S(2)}) copy-start(f32[16]{0:T(128)} %param.39) | copy-start | bytes 196
  0.7 19.7 %copy-start.10 = (bf16[2048,16]{0,1:T(8,128)(2,1)S(1)}, bf16[2048,16]{0,1:T(8,128)(2,1)}, u32[]{:S(2)}) copy-start(bf16[2048,16]{0,1:T(8,128)(2,1)} %param.35) | copy-start | bytes 196612
  0.7 19.7 %copy-start.13 = (f32[16]{0:T(128)S(1)}, f32[16]{0:T(128)}, u32[]{:S(2)}) copy-start(f32[16]{0:T(128)} %param.38) | copy-start | bytes 196
  0.7 19.7 %copy-start.12 = (f32[16]{0:T(128)S(1)}, f32[16]{0:T(128)}, u32[]{:S(2)}) copy-start(f32[16]{0:T(128)} %param.40) | copy-start | bytes 196
  0.7 19.9 %copy-start.3 = (f32[2,16,64,128]{3,2,1,0:T(8,128)S(1)}, f32[2,16,64,128]{3,2,1,0:T(8,128)}, u32[]{:S(2)}) copy-start(f32[2,16,64,128]{3,2,1,0:T(8,128)} %param.27) | copy-start | bytes 3145732
  2.6 24.4 %collective-permute-start = (bf16[56,2048]{1,0:T(8,128)(2,1)S(1)}, bf16[56,2048]{1,0:T(8,128)(2,1)S(1)}, u32[]{:S(2)}, u32[]{:S(2)}) collective-permute-start(bf16[56,2048]{1,0:T(8,128)(2,1)S(1)} %get-tuple-element.23.h0), channel_id=1, source_target_pairs={{0,6},{2,0},{4,2},{6,4},{1,7},{3,1},{5,3},{7,5},{8,14},{10,8},{12,... | collective-permute-start | bytes 688136 | tf_op jit(solution)/shard_map/ppermute | solution.py:36
  5.9 21.1 %collective-permute-start.1 = (bf16[56,2048]{1,0:T(8,128)(2,1)S(1)}, bf16[56,2048]{1,0:T(8,128)(2,1)S(1)}, u32[]{:S(2)}, u32[]{:S(2)}) collective-permute-start(bf16[56,2048]{1,0:T(8,128)(2,1)S(1)} %get-tuple-element.23.h0), channel_id=1, source_target_pairs={{0,4},{2,6},{4,0},{6,2},{1,5},{3,7},{5,1},{7,3},{8,12},{10,14},{12... | collective-permute-start | bytes 688136 | tf_op jit(solution)/shard_map/ppermute | solution.py:36
  6.4 20.6 %collective-permute-start.2 = (bf16[56,2048]{1,0:T(8,128)(2,1)S(1)}, bf16[56,2048]{1,0:T(8,128)(2,1)S(1)}, u32[]{:S(2)}, u32[]{:S(2)}) collective-permute-start(bf16[56,2048]{1,0:T(8,128)(2,1)S(1)} %get-tuple-element.23.h0), channel_id=1, source_target_pairs={{0,2},{2,4},{4,6},{6,0},{1,3},{3,5},{5,7},{7,1},{8,10},{10,12},{12... | collective-permute-start | bytes 688136 | tf_op jit(solution)/shard_map/ppermute | solution.py:36
  7.0 19.9 %all-to-all-start = ((bf16[32,2,256]{2,1,0:T(2,128)(2,1)}), bf16[32,2,256]{2,1,0:T(2,128)(2,1)S(1)}, u32[]{:S(2)}, u32[]{:S(2)}) async-start(bf16[32,2,256]{2,1,0:T(2,128)(2,1)} %get-tuple-element.22), calls=%async_computation | async-start | bytes 65536 | tf_op jit(solution)/shard_map/all_to_all | solution.py:31
  18.5 24.5 %copy-start.5 = (bf16[2,3,1024]{2,0,1:T(2,128)(2,1)S(1)}, bf16[2,3,1024]{2,0,1:T(2,128)(2,1)}, u32[]{:S(2)}) copy-start(bf16[2,3,1024]{2,0,1:T(2,128)(2,1)} %param.28) | copy-start | bytes 36868
  18.5 24.5 %copy-start.6 = (f32[4,1024]{1,0:T(4,128)S(1)}, f32[4,1024]{1,0:T(4,128)}, u32[]{:S(2)}) copy-start(f32[4,1024]{1,0:T(4,128)} %param.36) | copy-start | bytes 49156
  20.0 23.3 %copy-start.9 = (f32[1024]{0:T(1024)S(1)}, f32[1024]{0:T(1024)}, u32[]{:S(2)}) copy-start(f32[1024]{0:T(1024)} %param.41) | copy-start | bytes 12292
  28.1 52.3 %copy-start.1 = (f32[2048]{0:T(1024)S(1)}, f32[2048]{0:T(1024)}, u32[]{:S(2)}) copy-start(f32[2048]{0:T(1024)} %param.43) | copy-start | bytes 24580
  28.1 14.7 %all-to-all-start.1 = ((bf16[32,2,2048]{2,1,0:T(2,128)(2,1)}), bf16[32,2,2048]{2,1,0:T(2,128)(2,1)S(1)}, u32[]{:S(2)}, u32[]{:S(2)}) async-start(bf16[32,2,2048]{2,1,0:T(2,128)(2,1)} %in_part.1), calls=%async_computation.1 | async-start | bytes 524288 | tf_op jit(solution)/shard_map/all_to_all | solution.py:31
  32.2 52.7 %copy-start.2 = (f32[2048]{0:T(1024)S(1)}, f32[2048]{0:T(1024)}, u32[]{:S(2)}) copy-start(f32[2048]{0:T(1024)} %param.51) | copy-start | bytes 24580
  44.0 13.3 %all-to-all-start.2 = ((bf16[32,2,1024]{2,1,0:T(2,128)(2,1)}), bf16[32,2,1024]{2,1,0:T(2,128)(2,1)S(1)}, u32[]{:S(2)}, u32[]{:S(2)}) async-start(bf16[32,2,1024]{2,1,0:T(2,128)(2,1)} %broadcast_in_dim.46), calls=%async_computation.2 | async-start | bytes 262144 | tf_op jit(solution)/shard_map/all_to_all | solution.py:31
  57.7 6.0 %collective-permute-start.3 = (f32[64,64]{1,0:T(8,128)S(1)}, f32[64,64]{1,0:T(8,128)S(1)}, u32[]{:S(2)}, u32[]{:S(2)}) collective-permute-start(f32[64,64]{1,0:T(8,128)S(1)} %out_part.1.part), channel_id=1, source_target_pairs={{0,1},{1,0},{2,3},{3,2},{4,5},{5,4},{6,7},{7,6},{8,9},{9,8},{10,11... | collective-permute-start | bytes 49160 | tf_op jit(solution)/shard_map/ppermute | solution.py:36
  64.6 15.7 %all-to-all-start.3 = ((bf16[32,32,128]{2,1,0:T(8,128)(2,1)}), bf16[32,32,128]{2,1,0:T(8,128)(2,1)S(1)}, u32[]{:S(2)}, u32[]{:S(2)}) async-start(bf16[32,32,128]{2,1,0:T(8,128)(2,1)} %hidden_pieces.1), calls=%async_computation.3 | async-start | bytes 524288 | tf_op jit(solution)/shard_map/all_to_all | solution.py:31
  80.9 7.1 %collective-permute-start.4 = (bf16[32,2048]{1,0:T(8,128)(2,1)S(1)}, bf16[32,2048]{1,0:T(8,128)(2,1)S(1)}, u32[]{:S(2)}, u32[]{:S(2)}) collective-permute-start(bf16[32,2048]{1,0:T(8,128)(2,1)S(1)} %get-tuple-element.28), channel_id=1, source_target_pairs={{0,2},{2,4},{4,6},{6,0},{1,3},{3,5},{5,7},{7,1},{8,10},{10,12},{12... | collective-permute-start | bytes 393224 | tf_op jit(solution)/shard_map/ppermute | solution.py:36
  82.4 5.8 %collective-permute-start.5 = (bf16[32,2048]{1,0:T(8,128)(2,1)S(1)}, bf16[32,2048]{1,0:T(8,128)(2,1)S(1)}, u32[]{:S(2)}, u32[]{:S(2)}) collective-permute-start(bf16[32,2048]{1,0:T(8,128)(2,1)S(1)} %get-tuple-element.29), channel_id=1, source_target_pairs={{0,4},{2,6},{4,0},{6,2},{1,5},{3,7},{5,1},{7,3},{8,12},{10,14},{12... | collective-permute-start | bytes 393224 | tf_op jit(solution)/shard_map/ppermute | solution.py:36
  84.1 4.1 %collective-permute-start.6 = (bf16[32,2048]{1,0:T(8,128)(2,1)S(1)}, bf16[32,2048]{1,0:T(8,128)(2,1)S(1)}, u32[]{:S(2)}, u32[]{:S(2)}) collective-permute-start(bf16[32,2048]{1,0:T(8,128)(2,1)S(1)} %get-tuple-element.30), channel_id=1, source_target_pairs={{0,6},{2,0},{4,2},{6,4},{1,7},{3,1},{5,3},{7,5},{8,14},{10,8},{12,... | collective-permute-start | bytes 393224 | tf_op jit(solution)/shard_map/ppermute | solution.py:36
  90.7 19.9 %copy-start.4 = (f32[2,16,64,128]{3,2,1,0:T(8,128)S(1)}, f32[2,16,64,128]{3,2,1,0:T(8,128)}, u32[]{:S(2)}) copy-start(f32[2,16,64,128]{3,2,1,0:T(8,128)} %param.27) | copy-start | bytes 3145732
  90.7 5.5 %collective-permute-start.7 = (bf16[32,2048]{1,0:T(8,128)(2,1)S(1)}, bf16[32,2048]{1,0:T(8,128)(2,1)S(1)}, u32[]{:S(2)}, u32[]{:S(2)}) collective-permute-start(bf16[32,2048]{1,0:T(8,128)(2,1)S(1)} %get-tuple-element.34), channel_id=1, source_target_pairs={{0,6},{2,0},{4,2},{6,4},{1,7},{3,1},{5,3},{7,5},{8,14},{10,8},{12,... | collective-permute-start | bytes 393224 | tf_op jit(solution)/shard_map/ppermute | solution.py:36
  92.9 5.4 %collective-permute-start.8 = (bf16[32,2048]{1,0:T(8,128)(2,1)S(1)}, bf16[32,2048]{1,0:T(8,128)(2,1)S(1)}, u32[]{:S(2)}, u32[]{:S(2)}) collective-permute-start(bf16[32,2048]{1,0:T(8,128)(2,1)S(1)} %get-tuple-element.35), channel_id=1, source_target_pairs={{0,4},{2,6},{4,0},{6,2},{1,5},{3,7},{5,1},{7,3},{8,12},{10,14},{12... | collective-permute-start | bytes 393224 | tf_op jit(solution)/shard_map/ppermute | solution.py:36
  94.0 5.6 %collective-permute-start.9 = (bf16[32,2048]{1,0:T(8,128)(2,1)S(1)}, bf16[32,2048]{1,0:T(8,128)(2,1)S(1)}, u32[]{:S(2)}, u32[]{:S(2)}) collective-permute-start(bf16[32,2048]{1,0:T(8,128)(2,1)S(1)} %get-tuple-element.36), channel_id=1, source_target_pairs={{0,2},{2,4},{4,6},{6,0},{1,3},{3,5},{5,7},{7,1},{8,10},{10,12},{12... | collective-permute-start | bytes 393224 | tf_op jit(solution)/shard_map/ppermute | solution.py:36
  100.5 20.3 %all-to-all-start.4 = ((bf16[32,2,2048]{2,1,0:T(2,128)(2,1)}), bf16[32,2,2048]{2,1,0:T(2,128)(2,1)S(1)}, u32[]{:S(2)}, u32[]{:S(2)}) async-start(bf16[32,2,2048]{2,1,0:T(2,128)(2,1)} %terms.1), calls=%async_computation.4 | async-start | bytes 524288 | tf_op jit(solution)/shard_map/all_to_all | solution.py:31
  121.1 3.6 %collective-permute-start.10 = (f32[1,2048]{1,0:T(1,128)S(1)}, f32[1,2048]{1,0:T(1,128)S(1)}, u32[]{:S(2)}, u32[]{:S(2)}) collective-permute-start(f32[1,2048]{1,0:T(1,128)S(1)} %broadcast_select_fusion), channel_id=1, source_target_pairs={{0,1},{1,0},{2,3},{3,2},{4,5},{5,4},{6,7},{7,6},{8,9},{9,8},{10,11... | collective-permute-start | bytes 24584 | tf_op jit(solution)/shard_map/ppermute | solution.py:36
